TPU v7x, 256 devices: a whole 4x4x8 slice. The times are simulated.
256 devices in a mesh: ep: 64 (over z, x, core), tp: 4 (over y).
Axes of the slice: x: 4, y: 4, z: 8, core: 2. Of those that a mesh axis runs over, the one named last changes fastest.
Arguments:
- queries: bfloat16 [16384, 1024], P('ep', 'tp'), may hold values from -192 to 192
- keys_values: bfloat16 [16384, 512], P('ep', 'tp'), may hold values from -192 to 192
- log_gate_cum: float32 [16, 16384], P('tp'), as said below
- mix_weight: bfloat16 [1024, 2048], P('tp'), may hold values from -0.1875 to 0.1875
- mix_gain: float32 [2048], replicated, may hold values from 0.1 to 1.9
- moe_in: bfloat16 [49152, 2048], P(('ep', 'tp')), may hold values from -6 to 6
- moe_gain: float32 [2048], replicated, may hold values from 0.1 to 1.9
- routes: int32 [49152, 2], P(('ep', 'tp')), may hold values from 0 to 63, all different within a row; in each aligned block of 192 rows (0 to 191, 192 to 383, ...) at most 9 rows name the same one
- route_weight: float32 [49152, 2], P(('ep', 'tp')), may hold values from 0.25 to 2
- expert_gate: bfloat16 [64, 2048, 1024], P('ep', None, 'tp'), may hold values from -0.125 to 0.125
- expert_up: bfloat16 [64, 2048, 1024], P('ep', None, 'tp'), may hold values from -0.125 to 0.125
- expert_down: bfloat16 [64, 1024, 2048], P('ep', 'tp'), may hold values from -0.1875 to 0.1875
Outputs:
- mix_result: bfloat16 [16384, 2048], P(('ep', 'tp'))
- moe_result: bfloat16 [49152, 2048], P(('ep', 'tp'))
Inputs may be any that keep to these rules, and one draw needn't show every extreme that they name: `log_gate_cum`: along positions each head's values never rise. `routes`: each row names 2 different experts. Among the rows of one device no expert is named more than 9 times, and in every draw some device names some expert exactly 9 times.
All inputs are finite; a program needn't handle non-finite values.
Results may differ from a plain program's by a relative error of at most 0.013.
Values may be sent and summed in bfloat16 or wider, within the bound.
No kernel may reach another device: no remote copies, remote signals or barrier semaphores. Data moves between devices by JAX's collectives and lax.ppermute only.
A program may use at most 128 MiB of HBM per device.

v0:
```python
from functools import partial
import math

import jax
import jax.numpy as jnp
from jax import lax
from jax.sharding import PartitionSpec as P

HEAD = 64


EPSILON = 1e-06
NEGATIVE = -1e30


def sent_together(arrays, axis, dim, along):
    ends, at = ([], 0)
    for a in arrays[:-1]:
        at += a.shape[along]
        ends.append(at)
    both = jnp.concatenate(arrays, axis=along)
    return tuple(jnp.split(lax.all_gather(both, axis, axis=dim, tiled=True), ends, axis=along))


def cut_along(shard, dim, count):
    before, after = (shard.shape[:dim], shard.shape[dim + 1 :])
    return jnp.moveaxis(shard.reshape(*before, count, -1, *after), dim, 0)


def sum_at_owner(shard, axis, dim):
    count = lax.axis_size(axis)
    blocks = lax.all_to_all(cut_along(shard, dim, count), axis, 0, 0, tiled=True)
    return jnp.sum(blocks.astype(jnp.float32), axis=0)


def rms_scale(values, gain):
    widened = values.astype(jnp.float32)
    return widened * lax.rsqrt(jnp.mean(widened * widened, axis=-1, keepdims=True) + EPSILON) * gain


def slot_tables(route_block, experts, capacity):
    rows_here, top_picks = route_block.shape
    flat_routes = route_block.reshape(-1)
    onehot = (flat_routes[:, None] == jnp.arange(experts, dtype=jnp.int32)[None, :]).astype(
        jnp.int32
    )
    earlier = jnp.cumsum(onehot, axis=0) - onehot
    position = jnp.sum(earlier * onehot, axis=1)
    source_row = jnp.full((experts * capacity,), rows_here, jnp.int32)
    source_row = source_row.at[flat_routes * capacity + position].set(
        jnp.arange(rows_here * top_picks, dtype=jnp.int32) // top_picks
    )
    return (position.reshape(rows_here, top_picks), source_row)


def fold_update(grouped, query_pos, query_gate, key_block, key_gate, key_pos, running):
    running_max, row_total, summed = running
    scores = jnp.einsum(
        "tgrd,ngd->grtn", grouped, key_block[:, :, 0], preferred_element_type=jnp.float32
    ) * HEAD ** (-0.5)
    scores = scores + query_gate[..., None] - key_gate[:, :, None, :]
    causal = key_pos[None, :] <= query_pos[:, None]
    scores = jnp.where(causal, scores, NEGATIVE)
    new_max = jnp.maximum(running_max, jnp.max(scores, axis=-1))
    factor = jnp.exp(running_max - new_max)
    weight = jnp.where(causal, jnp.exp(scores - new_max[..., None]), 0.0)
    row_total = row_total * factor + jnp.sum(weight, axis=-1)
    summed = summed * factor[..., None] + jnp.einsum(
        "grtn,ngd->grtd",
        weight.astype(jnp.bfloat16),
        key_block[:, :, 1],
        preferred_element_type=jnp.float32,
    )
    return (new_max, row_total, summed)


def keep_state(running):
    return running


def gated_hidden(slot_rows, router_feature_lanes, up_columns):
    return (
        jax.nn.silu(jnp.dot(slot_rows, router_feature_lanes, preferred_element_type=jnp.float32))
        * jnp.dot(slot_rows, up_columns, preferred_element_type=jnp.float32)
    ).astype(jnp.bfloat16)


def body(
    queries,
    keys_values,
    log_gate_cum,
    mix_weight,
    mix_gain,
    moe_in,
    moe_gain,
    routes,
    route_weight,
    expert_gate,
    expert_up,
    expert_down,
):
    ep_count = lax.axis_size("ep")
    ep_index = lax.axis_index("ep")
    local_tokens = queries.shape[0]
    half_rows = local_tokens // 2
    offset = ep_index * local_tokens
    kv_local = keys_values.shape[1] // (2 * HEAD)
    heads_local = queries.shape[1] // HEAD
    group_size = heads_local // kv_local
    second_rows = queries[half_rows:]
    second_start = offset + half_rows

    def half_setup(rows, first_pos):
        grouped = rows.reshape(half_rows, kv_local, group_size, HEAD)
        query_pos = first_pos + jnp.arange(half_rows, dtype=jnp.int32)
        query_gate = lax.dynamic_slice_in_dim(log_gate_cum, first_pos, half_rows, 1)
        query_gate = query_gate.reshape(kv_local, group_size, half_rows)
        return (grouped, query_pos, query_gate, first_pos + half_rows - 1)

    halves = (half_setup(queries[:half_rows], offset), half_setup(second_rows, second_start))
    start_state = (
        jnp.full((kv_local, group_size, half_rows), NEGATIVE, jnp.float32),
        jnp.zeros((kv_local, group_size, half_rows), jnp.float32),
        jnp.zeros((kv_local, group_size, half_rows, HEAD), jnp.float32),
    )
    piece = lax.all_gather(keys_values, "ep", axis=0, tiled=True)
    piece_rows = piece.shape[0]
    block_rows = math.gcd(piece_rows, 512)

    def one_block(turn_index, fold_state):
        tile_opening = turn_index * block_rows
        key_block = lax.dynamic_slice_in_dim(piece, turn_index * block_rows, block_rows, 0)
        key_block = key_block.reshape(block_rows, kv_local, 2, HEAD)
        key_gate = lax.dynamic_slice_in_dim(log_gate_cum, tile_opening, block_rows, 1)
        key_gate = key_gate.reshape(kv_local, group_size, block_rows)
        key_pos = tile_opening + jnp.arange(block_rows, dtype=jnp.int32)
        updated = []
        for half_state, half_data in zip(fold_state, halves):
            grouped, query_pos, query_gate, last_query = half_data
            advance = partial(
                fold_update, grouped, query_pos, query_gate, key_block, key_gate, key_pos
            )
            updated.append(lax.cond(tile_opening <= last_query, advance, keep_state, half_state))
        return tuple(updated)

    folded = lax.fori_loop(0, piece_rows // block_rows, one_block, (start_state, start_state))

    def finish(state):
        _, row_total, summed = state
        mixed_heads = jnp.transpose(summed / row_total[..., None], (2, 0, 1, 3))
        return mixed_heads.reshape(half_rows, heads_local * HEAD).astype(jnp.bfloat16)

    first_done = finish(folded[0])
    second_done = finish(folded[1])
    attended = jnp.concatenate([first_done, second_done], axis=0)
    rows_here = moe_in.shape[0]
    top_picks = routes.shape[1]
    width_here = moe_in.shape[1]
    capacity = 3 * top_picks * rows_here // (2 * ep_count)
    normed = rms_scale(moe_in, moe_gain).astype(jnp.bfloat16)
    position, source_row = slot_tables(routes, ep_count, capacity)
    zero_row = jnp.zeros((1, width_here), jnp.bfloat16)
    down_here = expert_down[0]
    padded = jnp.concatenate([normed, zero_row], axis=0)
    received_rows = lax.all_to_all(
        padded[source_row].reshape(ep_count, capacity, width_here),
        "ep",
        split_axis=0,
        concat_axis=0,
        tiled=True,
    )
    slot_rows = received_rows.reshape(-1, width_here)
    slot_count = slot_rows.shape[0]
    pieces = sent_together((expert_gate[0], expert_up[0]), "tp", 1, 0)
    columns = gated_hidden(slot_rows, pieces[0], pieces[1])
    hidden = columns
    shard_rows = down_here.shape[0]
    total = jnp.zeros((slot_count, width_here), jnp.float32)
    add_piece = lax.all_gather(down_here, "tp", axis=0, tiled=True)
    for part_index in range(add_piece.shape[0] // shard_rows):
        columns = lax.dynamic_slice_in_dim(hidden, part_index * shard_rows, shard_rows, 1)
        width_part = jnp.dot(
            columns,
            add_piece[part_index * shard_rows : (part_index + 1) * shard_rows],
            preferred_element_type=jnp.float32,
        ).astype(jnp.bfloat16)
        total = total + lax.optimization_barrier(width_part).astype(jnp.float32)
    mix_sum = sum_at_owner(
        jnp.dot(attended, mix_weight, preferred_element_type=jnp.float32).astype(jnp.bfloat16),
        "tp",
        0,
    )
    mix_result = rms_scale(mix_sum, mix_gain).astype(jnp.bfloat16)
    expert_out = total.astype(jnp.bfloat16).reshape(ep_count, capacity, width_here)
    returned = lax.all_to_all(expert_out, "ep", split_axis=0, concat_axis=0, tiled=True).reshape(
        -1, width_here
    )
    chosen = returned[routes * capacity + position].astype(jnp.float32)
    moe_result = jnp.sum(route_weight[..., None] * chosen, axis=1).astype(jnp.bfloat16)
    return (mix_result, moe_result)


def solution(mesh):
    in_specs = (
        P("ep", "tp"),
        P("ep", "tp"),
        P("tp", None),
        P("tp", None),
        P(),
        P(("ep", "tp"), None),
        P(),
        P(("ep", "tp"), None),
        P(("ep", "tp"), None),
        P("ep", None, "tp"),
        P("ep", None, "tp"),
        P("ep", "tp", None),
    )
    out_specs = (P(("ep", "tp"), None), P(("ep", "tp"), None))
    return jax.shard_map(body, mesh=mesh, in_specs=in_specs, out_specs=out_specs, check_vma=False)
```

profile of v0, /device:TPU:8, one launch (start us, length us, event | category | flops | bytes accessed | tf_op | source)
XLA Modules:
  0.0 433.1 jit_solution(6988388845810025576)
XLA Ops:
  7.2 1.7 copy.22
  9.0 3.1 pad_maximum_fusion
  14.7 2.9 scatter_custom_fusion
  17.7 4.1 gather_fusion
  21.8 4.6 %reshape.184 = bf16[64,9,2048]{2,1,0:T(8,128)(2,1)} reshape(bf16[576,2048]{1,0:T(8,128)(2,1)} %gather_fusion) | data formatting | bytes 4718592 | tf_op jit(solution)/shard_map/reshape | solution.py:166
  26.4 12.3 %all-to-all-start.1 = ((bf16[64,9,2048]{2,1,0:T(8,128)(2,1)}), bf16[64,9,2048]{2,1,0:T(8,128)(2,1)}, u32[]{:S(2)}, u32[]{:S(2)}) async-start(bf16[64,9,2048]{2,1,0:T(8,128)(2,1)} %reshape.184), calls=%async_computation.1 | async-start | bytes 8388608 | tf_op jit(solution)/shard_map/all_to_all | solution.py:165
  40.4 102.9 %all-to-all-done.1 = bf16[64,9,2048]{2,1,0:T(8,128)(2,1)} async-done(((bf16[64,9,2048]{2,1,0:T(8,128)(2,1)}), bf16[64,9,2048]{2,1,0:T(8,128)(2,1)}, u32[]{:S(2)}, u32[]{:S(2)}) %all-to-all-start.1) | async-done | bytes 2359328 | tf_op jit(solution)/shard_map/all_to_all | solution.py:165
  143.4 4.9 %reshape.185 = bf16[576,2048]{1,0:T(8,128)(2,1)} reshape(bf16[64,9,2048]{2,1,0:T(8,128)(2,1)} %all-to-all-done.1) | data formatting | bytes 4718592 | tf_op jit(solution)/shard_map/reshape | solution.py:172
  148.4 56.5 %while.24 = (s32[]{:T(128)}, f32[1,4,128]{2,1,0:T(4,128)S(1)}, f32[1,4,128]{2,1,0:T(4,128)S(1)}, f32[1,4,128,64]{2,3,1,0:T(8,128)S(1)}, f32[1,4,128]{2,1,0:T(4,1...) while((s32[]{:T(128)}, f32[1,4,128]{2,1,0:T(4,128)S(1)}, ...), condition=%wide.region_9.10_spmd.clone, body=%wide.region_0.9_spmd.clone.sunk | while | flops 140250880 | bytes 8108587 | solution.py:146
  206.4 5.7 %all-to-all-start = ((bf16[4,64,2048]{2,1,0:T(8,128)(2,1)}), bf16[4,64,2048]{2,1,0:T(8,128)(2,1)S(1)}, u32[]{:S(2)}, u32[]{:S(2)}) async-start(bf16[4,64,2048]{2,1,0:T(8,128)(2,1)} %bitcast.34), calls=%async_computation | async-start | bytes 2097152 | tf_op jit(solution)/shard_map/all_to_all | solution.py:32
  212.1 12.1 %all-gather.7.cloned.1.call-done = bf16[4096,1024]{1,0:T(8,128)(2,1)} async-done(((bf16[4096,256]{1,0:T(8,128)(2,1)}), bf16[4096,1024]{1,0:T(8,128)(2,1)}) %all-gather.7.cloned.1.call-update) | async-done | bytes 8388624 | tf_op jit(solution)/shard_map/all_gather | solution.py:22
  224.2 4.5 %fusion.44 = f32[576,1024]{1,0:T(8,128)S(1)} fusion(bf16[576,2048]{1,0:T(8,128)(2,1)S(1)} %copy-done.5, bf16[4096,1024]{1,0:T(8,128)(2,1)} %all-gather.7.cloned.1.call-done), kind=kOutput, calls=%fused_computation.63 | convolution fusion | flops 2415919104 | bytes 8912896 | tf_op jit(solution)/shard_map/dot_general | solution.py:83
  228.9 3.8 multiply_convert_fusion
  232.6 39.1 %all-gather.9.cloned.1.call-done = bf16[1,1024,2048]{2,1,0:T(8,128)(2,1)} async-done(((bf16[1,256,2048]{2,1,0:T(8,128)(2,1)}), bf16[1,1024,2048]{2,1,0:T(8,128)(2,1)}) %all-gather.9.cloned.1.call-update) | async-done | bytes 4194320 | tf_op jit(solution)/shard_map/all_gather | solution.py:179
  271.7 2.2 convolution_convert_fusion.3
  273.9 2.0 convolution_convert_fusion.2
  277.6 2.1 add_convert_fusion
  279.7 2.8 reshape.186
  283.5 27.9 %all-to-all-start.2 = ((bf16[64,9,2048]{2,1,0:T(8,128)(2,1)}), bf16[64,9,2048]{2,1,0:T(8,128)(2,1)}, u32[]{:S(2)}, u32[]{:S(2)}) async-start(bf16[64,9,2048]{2,1,0:T(8,128)(2,1)} %reshape.186), calls=%async_computation.2 | async-start | bytes 8388608 | tf_op jit(solution)/shard_map/all_to_all | solution.py:195
  314.1 93.3 %all-to-all-done.2 = bf16[64,9,2048]{2,1,0:T(8,128)(2,1)} async-done(((bf16[64,9,2048]{2,1,0:T(8,128)(2,1)}), bf16[64,9,2048]{2,1,0:T(8,128)(2,1)}, u32[]{:S(2)}, u32[]{:S(2)}) %all-to-all-start.2) | async-done | bytes 2359328 | tf_op jit(solution)/shard_map/all_to_all | solution.py:195
  407.4 3.4 reshape.187
  410.8 3.1 gather_fusion.1
  413.9 4.8 %reshape.221 = f32[192,2,2048]{2,1,0:T(2,128)} reshape(bf16[384,2048]{1,0:T(8,128)(2,1)} %gather_fusion.1) | data formatting | bytes 4718592 | tf_op jit(solution)/shard_map/convert_element_type | solution.py:198
  418.8 7.8 %multiply_reduce_fusion = bf16[192,2048]{1,0:T(8,128)(2,1)} fusion(f32[192,2,2048]{2,1,0:T(2,128)} %reshape.221, f32[192,2]{1,0:T(8,128)S(1)} %copy.25), kind=kLoop, calls=%fused_computation.65 | loop fusion | flops 1179648 | bytes 3933696 | tf_op jit(solution)/shard_map/reduce_sum | solution.py:199
  (314 shorter events, 68.7 us)
Async XLA Ops:
  7.2 197.8 %copy-start = (bf16[256,2048]{1,0:T(8,128)(2,1)S(1)}, bf16[256,2048]{1,0:T(8,128)(2,1)}, u32[]{:S(2)}) copy-start(bf16[256,2048]{1,0:T(8,128)(2,1)} %param.21) | copy-start | bytes 3145732
  7.2 141.1 %all-gather.5.cloned.1.call-start = ((), (), s32[]{:S(2)}) async-start(), calls=%async_computation.3 | async-start | bytes 4259840 | tf_op jit(solution)/shard_map/all_gather | solution.py:126
  8.9 215.3 %all-gather.7.cloned.1.call-start = ((), (), s32[]{:S(2)}) async-start(), calls=%async_computation.4 | async-start | bytes 10485760 | tf_op jit(solution)/shard_map/all_gather | solution.py:22
  9.0 3.1 copy-start.10
  12.0 2.1 copy-start.4
  12.0 2.3 copy-start.8
  26.4 13.1 %copy-start.7 = (bf16[256,256]{1,0:T(8,128)(2,1)S(1)}, bf16[256,256]{1,0:T(8,128)(2,1)}, u32[]{:S(2)}) copy-start(bf16[256,256]{1,0:T(8,128)(2,1)} %param.18) | copy-start | bytes 393220
  26.4 117.0 %all-to-all-start.1 = ((bf16[64,9,2048]{2,1,0:T(8,128)(2,1)}), bf16[64,9,2048]{2,1,0:T(8,128)(2,1)}, u32[]{:S(2)}, u32[]{:S(2)}) async-start(bf16[64,9,2048]{2,1,0:T(8,128)(2,1)} %reshape.184), calls=%async_computation.1 | async-start | bytes 8388608 | tf_op jit(solution)/shard_map/all_to_all | solution.py:165
  38.7 232.9 %all-gather.9.cloned.1.call-start = ((), (), s32[]{:S(2)}) async-start(), calls=%async_computation.5 | async-start | bytes 5242880 | tf_op jit(solution)/shard_map/all_gather | solution.py:179
  204.9 19.3 %copy-start.5 = (bf16[576,2048]{1,0:T(8,128)(2,1)S(1)}, bf16[576,2048]{1,0:T(8,128)(2,1)}, u32[]{:S(2)}) copy-start(bf16[576,2048]{1,0:T(8,128)(2,1)} %reshape.185) | copy-start | bytes 7077892
  206.4 76.1 %all-to-all-start = ((bf16[4,64,2048]{2,1,0:T(8,128)(2,1)}), bf16[4,64,2048]{2,1,0:T(8,128)(2,1)S(1)}, u32[]{:S(2)}, u32[]{:S(2)}) async-start(bf16[4,64,2048]{2,1,0:T(8,128)(2,1)} %bitcast.34), calls=%async_computation | async-start | bytes 2097152 | tf_op jit(solution)/shard_map/all_to_all | solution.py:32
  224.2 4.6 %copy-start.12 = (bf16[4096,1024]{1,0:T(8,128)(2,1)S(1)}, bf16[4096,1024]{1,0:T(8,128)(2,1)}, u32[]{:S(2)}) copy-start(bf16[4096,1024]{1,0:T(8,128)(2,1)} %all-gather.7.cloned.1.call-done) | copy-start | bytes 25165828
  232.6 41.3 %copy-start.6 = (bf16[576,1024]{1,0:T(8,128)(2,1)S(1)}, bf16[576,1024]{1,0:T(8,128)(2,1)}, u32[]{:S(2)}) copy-start(bf16[576,1024]{1,0:T(8,128)(2,1)} %multiply_convert_fusion) | copy-start | bytes 3538948
  271.7 4.3 copy-start.2
  282.5 29.1 %copy-start.11 = (f32[192,2]{0,1:T(2,128)S(1)}, f32[192,2]{0,1:T(2,128)}, u32[]{:S(2)}) copy-start(f32[192,2]{0,1:T(2,128)} %param.26) | copy-start | bytes 4612
  282.5 30.8 %copy-start.9 = (f32[2048]{0:T(1024)S(1)}, f32[2048]{0:T(1024)}, u32[]{:S(2)}) copy-start(f32[2048]{0:T(1024)} %param.22) | copy-start | bytes 24580
  282.5 1.1 copy-start.3
  283.5 123.9 %all-to-all-start.2 = ((bf16[64,9,2048]{2,1,0:T(8,128)(2,1)}), bf16[64,9,2048]{2,1,0:T(8,128)(2,1)}, u32[]{:S(2)}, u32[]{:S(2)}) async-start(bf16[64,9,2048]{2,1,0:T(8,128)(2,1)} %reshape.186), calls=%async_computation.2 | async-start | bytes 8388608 | tf_op jit(solution)/shard_map/all_to_all | solution.py:195
  413.9 12.6 %copy-start.1 = (bf16[256,2048]{1,0:T(8,128)(2,1)S(1)}, bf16[256,2048]{1,0:T(8,128)(2,1)}, u32[]{:S(2)}) copy-start(bf16[256,2048]{1,0:T(8,128)(2,1)} %param.21) | copy-start | bytes 3145732
Sparse Core Ops, SparseCore 0:
  11.2 117.0 all-gather.4
  130.1 94.1 all-gather.6
  226.0 45.6 all-gather.8
where the time goes:
time: 436 us; the launch traced here: 433 us
  waiting for transfers between devices  248 us (57%)
  local copies, waits for them, and re-layouts  87.9 us (20%)
  starting transfers between devices  46 us (11%)
  other arithmetic  17.9 us (4%)
  matrix products  17.1 us (4%)
  between operations  14.1 us (3%)
    all_to_all x1, waiting for transfers between devices, body(): lax.all_to_all(padded[source_row].reshape(ep_count, capacity, width_here)...  103 us
    all_to_all x1, waiting for transfers between devices, body(): lax.all_to_all(expert_out, 'ep', split_axis=0, concat_axis=0, tiled=True)  93.3 us
    all_gather x1, waiting for transfers between devices, body(): add_piece = lax.all_gather(down_here, 'tp', axis=0, tiled=True)  39.1 us
    dynamic_slice x32, local copies, waits for them, and re-layouts, one_block(): lax.dynamic_slice_in_dim(piece, turn_index * block_rows, block_rows, 0)  29.5 us
    all_to_all x1, starting transfers between devices, body(): lax.all_to_all(expert_out, 'ep', split_axis=0, concat_axis=0, tiled=True)  27.9 us
    dynamic_slice x32, local copies, waits for them, and re-layouts, one_block(): lax.dynamic_slice_in_dim(log_gate_cum, tile_opening, block_rows, 1)  22.6 us
    all_to_all x1, starting transfers between devices, body(): lax.all_to_all(padded[source_row].reshape(ep_count, capacity, width_here)...  12.3 us
    all_gather x1, waiting for transfers between devices, sent_together(): lax.all_gather(both, axis, axis=dim, tiled=True)  12.1 us
  transfers between devices with their start and end apart: 6, of which 4 were waited for; matrix products, arithmetic and copies ran while one was open for 23% of the time, Pallas kernels for 0%

commit v1 on v0

v1 whole, which is shorter than its diff:
```python
import jax
import jax.numpy as jnp
from jax import lax
from jax.experimental import pallas as pl
from jax.experimental.pallas import tpu as pltpu
from jax.sharding import PartitionSpec as P


HEAD = 64
EPSILON = 1e-06
NEGATIVE = -1e30
LANES = 256
KEY_BLOCK = 1024
LOG2E = 1.4426950408889634


def slot_positions(routes, experts):
    tokens = routes.shape[1]
    first, second = routes[0:1, :], routes[1:2, :]
    expert_ids = lax.broadcasted_iota(jnp.int32, (experts, tokens), 0)
    one_first = (first == expert_ids).astype(jnp.float32)
    one_second = (second == expert_ids).astype(jnp.float32)
    row = lax.broadcasted_iota(jnp.int32, (tokens, tokens), 0)
    col = lax.broadcasted_iota(jnp.int32, (tokens, tokens), 1)
    earlier = (row < col).astype(jnp.float32).astype(jnp.bfloat16)
    count_first = jnp.dot(
        one_first.astype(jnp.bfloat16), earlier, preferred_element_type=jnp.float32
    )
    count_second = jnp.dot(
        one_second.astype(jnp.bfloat16), earlier, preferred_element_type=jnp.float32
    ) + jnp.sum(one_first, axis=1, keepdims=True)
    place_first = jnp.sum(one_first * count_first, axis=0, keepdims=True).astype(jnp.int32)
    place_second = jnp.sum(one_second * count_second, axis=0, keepdims=True).astype(jnp.int32)
    return (first, place_first), (second, place_second)


def slot_masks(expert, place, experts):
    tokens = expert.shape[1]
    eight = lax.broadcasted_iota(jnp.int32, (experts * 8, tokens), 0)
    ninth = lax.broadcasted_iota(jnp.int32, (experts, tokens), 0)
    in_eight = eight == jnp.where(place < 8, expert * 8 + place, -1)
    in_ninth = ninth == jnp.where(place == 8, expert, -1)
    return in_eight, in_ninth


def as_bf16(mask):
    return mask.astype(jnp.float32).astype(jnp.bfloat16)


def as_rows(block):
    wide = block.astype(jnp.float32)
    return wide.reshape(-1, block.shape[-1]).astype(jnp.bfloat16)


def dispatch_kernel(routes_ref, tokens_ref, out_ref, ninth_ref):
    experts = out_ref.shape[0]
    groups = tokens_ref.shape[1] // LANES
    picks = slot_positions(routes_ref[...], experts)
    (a8, a9), (b8, b9) = [slot_masks(e, p, experts) for e, p in picks]
    pick8 = as_bf16(jnp.logical_or(a8, b8))
    pick9 = as_bf16(jnp.logical_or(a9, b9))
    for g in range(groups):
        columns = tokens_ref[:, g * LANES : (g + 1) * LANES]
        chosen = jnp.dot(pick8, columns, preferred_element_type=jnp.float32)
        out_ref[:, g * 8 : (g + 1) * 8, :] = chosen.reshape(experts, 8, LANES).astype(jnp.bfloat16)
        last = jnp.dot(pick9, columns, preferred_element_type=jnp.float32)
        for half in range(LANES // 128):
            ninth_ref[half, pl.ds(g, experts, stride=groups), :] = last[
                :, half * 128 : (half + 1) * 128
            ]
    whole = jnp.concatenate([ninth_ref[half] for half in range(LANES // 128)], axis=1)
    out_ref[:, 8 * groups :, :] = whole.reshape(experts, groups, LANES).astype(jnp.bfloat16)


def hidden_kernel(
    received_ref, gain_ref,
    g0, u0, g1, u1, g2, u2, g3, u3,
    hidden_ref,
    gate_buf, up_buf, tokens_ref, ninth_ref, sems,
):
    sources = received_ref.shape[0]
    groups = received_ref.shape[1] // 9
    width = groups * LANES
    eights = sources * 8
    ff = g0.shape[1]
    copies = []
    for n, (g, u) in enumerate(((g0, u0), (g1, u1), (g2, u2), (g3, u3))):
        copies.append(pltpu.make_async_copy(g, gate_buf.at[n], sems.at[2 * n]))
        copies.append(pltpu.make_async_copy(u, up_buf.at[n], sems.at[2 * n + 1]))
    for c in copies:
        c.start()

    ninth = received_ref[:, 8 * groups :, :].astype(jnp.float32).reshape(sources * groups, LANES)
    for h in range(LANES // 128):
        ninth_ref[h] = ninth[:, h * 128 : (h + 1) * 128]

    def eight_rows(g):
        block = received_ref[:, g * 8 : (g + 1) * 8, :].astype(jnp.float32)
        return block.reshape(eights, LANES)

    def ninth_rows(g):
        return jnp.concatenate(
            [ninth_ref[h, pl.ds(g, sources, stride=groups), :] for h in range(LANES // 128)], axis=1
        )

    square8 = jnp.zeros((eights, LANES), jnp.float32)
    square9 = jnp.zeros((sources, LANES), jnp.float32)
    for g in range(groups):
        x = eight_rows(g)
        square8 = square8 + x * x
        y = ninth_rows(g)
        square9 = square9 + y * y
    scale8 = lax.rsqrt(jnp.sum(square8, axis=1, keepdims=True) / width + EPSILON)
    scale9 = lax.rsqrt(jnp.sum(square9, axis=1, keepdims=True) / width + EPSILON)
    for g in range(groups):
        gain = gain_ref[:, g * LANES : (g + 1) * LANES]
        tokens_ref[:eights, g * LANES : (g + 1) * LANES] = (
            eight_rows(g) * scale8 * gain
        ).astype(jnp.bfloat16)
        tokens_ref[eights:, g * LANES : (g + 1) * LANES] = (
            ninth_rows(g) * scale9 * gain
        ).astype(jnp.bfloat16)

    for n in range(4):
        copies[2 * n].wait()
        copies[2 * n + 1].wait()
        gated = jnp.dot(tokens_ref[...], gate_buf[n], preferred_element_type=jnp.float32)
        lifted = jnp.dot(tokens_ref[...], up_buf[n], preferred_element_type=jnp.float32)
        hidden_ref[:, n * ff : (n + 1) * ff] = (
            gated / (1.0 + jnp.exp(-gated)) * lifted
        ).astype(jnp.bfloat16)


def down_kernel(hidden_ref, d0, d1, d2, d3a, d3b, out_ref, down_buf, ninth_ref, sems):
    sources = out_ref.shape[0]
    groups = out_ref.shape[1] // 9
    eights = sources * 8
    ff = d0.shape[0]
    half = d3a.shape[0]
    pieces = ((d0, 0, ff), (d1, ff, ff), (d2, 2 * ff, ff), (d3a, 3 * ff, half), (d3b, 3 * ff + half, half))
    copies = []
    for g in range(groups):
        columns = pl.ds(g * LANES, LANES)
        copies.append(
            [
                pltpu.make_async_copy(
                    d.at[:, columns], down_buf.at[g, pl.ds(at, size), :], sems.at[5 * g + n]
                )
                for n, (d, at, size) in enumerate(pieces)
            ]
        )
    for group in copies:
        for c in group:
            c.start()
    for g in range(groups):
        for c in copies[g]:
            c.wait()
        result = jnp.dot(hidden_ref[...], down_buf[g], preferred_element_type=jnp.float32)
        out_ref[:, g * 8 : (g + 1) * 8, :] = (
            result[:eights].reshape(sources, 8, LANES).astype(jnp.bfloat16)
        )
        for h in range(LANES // 128):
            ninth_ref[h, pl.ds(g, sources, stride=groups), :] = result[
                eights:, h * 128 : (h + 1) * 128
            ]
    whole = jnp.concatenate([ninth_ref[h] for h in range(LANES // 128)], axis=1)
    out_ref[:, 8 * groups :, :] = whole.reshape(sources, groups, LANES).astype(jnp.bfloat16)


def attention_kernel(
    place_ref, queries_ref, keys_ref, gate_ref, mix_ref, after_ref,
    own_ref, right_ref, left_ref, far_ref,
    scaled_ref, sums_ref, top_ref, mixed_ref,
):
    rows = queries_ref.shape[0]
    heads = queries_ref.shape[1] // HEAD
    block = min(KEY_BLOCK, keys_ref.shape[0])
    quarter = own_ref.shape[0]
    first_row = place_ref[0] * rows
    for h in range(heads):
        part = queries_ref[:, h * HEAD : (h + 1) * HEAD].astype(jnp.float32) * HEAD ** (-0.5)
        scaled_ref[h] = jnp.concatenate([part, jnp.zeros_like(part)], axis=1).astype(jnp.bfloat16)
    sums_ref[...] = jnp.zeros_like(sums_ref)
    top_ref[...] = jnp.full_like(top_ref, NEGATIVE)
    value_lane = lax.broadcasted_iota(jnp.int32, (block, 2 * HEAD), 1) >= HEAD

    def fold(start, masked):
        pairs = keys_ref[pl.ds(start, block), :]
        values = jnp.where(value_lane, pairs.astype(jnp.float32), 1.0).astype(jnp.bfloat16)
        if masked:
            query_pos = first_row + lax.broadcasted_iota(jnp.int32, (rows, block), 0)
            key_pos = start + lax.broadcasted_iota(jnp.int32, (rows, block), 1)
            causal = key_pos <= query_pos
        scores = [
            lax.dot_general(
                scaled_ref[h], pairs, (((1,), (1,)), ((), ())), preferred_element_type=jnp.float32
            )
            * LOG2E
            - gate_ref[h : h + 1, pl.ds(start, block)] * LOG2E
            for h in range(heads)
        ]
        folded = []
        for h in range(heads):
            score = scores[h]
            if masked:
                score = jnp.where(causal, score, NEGATIVE)
            old_top = top_ref[h][:, 0:1]
            new_top = jnp.maximum(old_top, jnp.max(score, axis=1, keepdims=True))
            weight = jnp.exp2(score - new_top)
            if masked:
                weight = jnp.where(causal, weight, 0.0)
            top_ref[h] = jnp.broadcast_to(new_top, top_ref.shape[1:])
            folded.append((weight.astype(jnp.bfloat16), jnp.exp2(old_top - new_top)))
        for h in range(heads):
            weight, kept = folded[h]
            sums_ref[h] = sums_ref[h] * kept + jnp.dot(
                weight, values, preferred_element_type=jnp.float32
            )

    whole_blocks = first_row // block

    def step(i, carry):
        fold(pl.multiple_of(i * block, block), False)
        return carry

    lax.fori_loop(0, whole_blocks, step, 0)
    fold(pl.multiple_of(whole_blocks * block, block), True)
    mixed = []
    for h in range(heads):
        total = sums_ref[h]
        mixed.append(total[:, HEAD:] / total[:, 0:1])
    mixed_ref[...] = jnp.concatenate(mixed, axis=1).astype(jnp.bfloat16)
    parts = 4
    for shift, out_ref in ((0, own_ref), (1, right_ref), (3, left_ref), (2, far_ref)):
        at = pl.multiple_of(((place_ref[1] + shift) % parts) * quarter, quarter)
        out_ref[...] = jnp.dot(
            mixed_ref[pl.ds(at, quarter), :], mix_ref[...], preferred_element_type=jnp.float32
        ).astype(jnp.bfloat16)


def combine_kernel(routes_ref, weight_ref, returned_ref, out_ref, ninth_ref):
    experts = returned_ref.shape[0]
    groups = returned_ref.shape[1] // 9
    tokens = routes_ref.shape[1]
    picks = slot_positions(routes_ref[...], experts)
    masks = [[as_bf16(m) for m in slot_masks(e, p, experts)] for e, p in picks]
    row = lax.broadcasted_iota(jnp.int32, (tokens, tokens), 0)
    col = lax.broadcasted_iota(jnp.int32, (tokens, tokens), 1)
    weights = [
        jnp.sum(jnp.where(row == col, weight_ref[k : k + 1, :], 0.0), axis=1, keepdims=True)
        for k in range(2)
    ]
    ninth = returned_ref[:, 8 * groups :, :].astype(jnp.float32).reshape(experts * groups, LANES)
    for h in range(LANES // 128):
        ninth_ref[h] = ninth[:, h * 128 : (h + 1) * 128]
    over_slots = (((0,), (0,)), ((), ()))
    for g in range(groups):
        eight = as_rows(returned_ref[:, g * 8 : (g + 1) * 8, :])
        last = jnp.concatenate(
            [ninth_ref[h, pl.ds(g, experts, stride=groups), :] for h in range(LANES // 128)], axis=1
        ).astype(jnp.bfloat16)
        total = 0.0
        for k in range(2):
            chosen = lax.dot_general(
                masks[k][0], eight, over_slots, preferred_element_type=jnp.float32
            ) + lax.dot_general(masks[k][1], last, over_slots, preferred_element_type=jnp.float32)
            total = total + weights[k] * chosen
        out_ref[:, g * LANES : (g + 1) * LANES] = total.astype(jnp.bfloat16)


def rms_scale(values, gain):
    return values * lax.rsqrt(jnp.mean(values * values, axis=-1, keepdims=True) + EPSILON) * gain


VMEM = pl.BlockSpec(memory_space=pltpu.VMEM)
SMEM = pl.BlockSpec(memory_space=pltpu.SMEM)
ANY = pl.BlockSpec(memory_space=pl.ANY)


def body(
    queries,
    keys_values,
    log_gate_cum,
    mix_weight,
    mix_gain,
    moe_in,
    moe_gain,
    routes,
    route_weight,
    expert_gate,
    expert_up,
    expert_down,
):
    ep_count = lax.axis_size("ep")
    tp_count = lax.axis_size("tp")
    place = jnp.stack([lax.axis_index("ep"), lax.axis_index("tp")]).astype(jnp.int32)
    to_right = [(i, (i + 1) % tp_count) for i in range(tp_count)]
    to_left = [(i, (i - 1) % tp_count) for i in range(tp_count)]
    to_far = [(i, (i + 2) % tp_count) for i in range(tp_count)]
    rows_here, width = moe_in.shape
    groups = width // LANES
    slot_rows = ep_count * 9
    ff = expert_gate.shape[2]
    lane_routes, lane_weight = routes.T, route_weight.T

    gate, up, down = expert_gate[0], expert_up[0], expert_down[0]
    gate_r = lax.ppermute(gate, "tp", to_right)
    up_l = lax.ppermute(up, "tp", to_left)
    up_r = lax.ppermute(up, "tp", to_right)
    gate_l = lax.ppermute(gate, "tp", to_left)
    gate_f = lax.ppermute(gate_r, "tp", to_right)
    up_f = lax.ppermute(up_l, "tp", to_left)
    down_r = lax.ppermute(down, "tp", to_right)
    down_l = lax.ppermute(down, "tp", to_left)
    down_fa = lax.ppermute(down_r[: ff // 2], "tp", to_right)
    down_fb = lax.ppermute(down_l[ff // 2 :], "tp", to_left)

    all_pairs = lax.all_gather(keys_values, "ep", axis=0, tiled=True)

    exchange_shape = jax.ShapeDtypeStruct((ep_count, 9 * groups, LANES), jnp.bfloat16)
    outgoing = pl.pallas_call(
        dispatch_kernel,
        out_shape=exchange_shape,
        in_specs=[VMEM, VMEM],
        out_specs=VMEM,
        scratch_shapes=[pltpu.VMEM((LANES // 128, ep_count * groups, 128), jnp.float32)],
        name="dispatch_rows",
    )(lane_routes, moe_in)
    received = lax.all_to_all(outgoing, "ep", 0, 0, tiled=True)
    hidden = pl.pallas_call(
        hidden_kernel,
        out_shape=jax.ShapeDtypeStruct((slot_rows, tp_count * ff), jnp.bfloat16),
        in_specs=[VMEM, VMEM] + [ANY] * 8,
        out_specs=VMEM,
        scratch_shapes=[
            pltpu.VMEM((tp_count, width, ff), jnp.bfloat16),
            pltpu.VMEM((tp_count, width, ff), jnp.bfloat16),
            pltpu.VMEM((slot_rows, width), jnp.bfloat16),
            pltpu.VMEM((LANES // 128, ep_count * groups, 128), jnp.float32),
            pltpu.SemaphoreType.DMA((8,)),
        ],
        cost_estimate=pl.CostEstimate(
            flops=4 * slot_rows * width * ff * tp_count,
            bytes_accessed=12_000_000,
            transcendentals=0,
        ),
        name="hidden_rows",
    )(
        received, moe_gain.reshape(1, width),
        gate, up, gate_r, up_r, gate_l, up_l, gate_f, up_f,
    )
    results = pl.pallas_call(
        down_kernel,
        out_shape=exchange_shape,
        in_specs=[VMEM] + [ANY] * 5,
        out_specs=VMEM,
        scratch_shapes=[
            pltpu.VMEM((groups, tp_count * ff, LANES), jnp.bfloat16),
            pltpu.VMEM((LANES // 128, ep_count * groups, 128), jnp.float32),
            pltpu.SemaphoreType.DMA((5 * groups,)),
        ],
        cost_estimate=pl.CostEstimate(
            flops=2 * slot_rows * width * ff * tp_count,
            bytes_accessed=8_000_000,
            transcendentals=0,
        ),
        name="down_rows",
    )(hidden, down, down_r, down_l, down_fa, down_fb)
    returned = lax.all_to_all(results, "ep", 0, 0, tiled=True)
    rows, head_width = queries.shape
    heads = head_width // HEAD
    quarter = rows // tp_count
    quarter_shape = jax.ShapeDtypeStruct((quarter, width), jnp.bfloat16)
    own, right, left, far = pl.pallas_call(
        attention_kernel,
        out_shape=[quarter_shape] * 4,
        in_specs=[SMEM, VMEM, VMEM, VMEM, VMEM, ANY],
        out_specs=[VMEM] * 4,
        scratch_shapes=[
            pltpu.VMEM((heads, rows, 2 * HEAD), jnp.bfloat16),
            pltpu.VMEM((heads, rows, 2 * HEAD), jnp.float32),
            pltpu.VMEM((heads, rows, 128), jnp.float32),
            pltpu.VMEM((rows, head_width), jnp.bfloat16),
        ],
        cost_estimate=pl.CostEstimate(
            flops=30_000_000_000, bytes_accessed=5_000_000, transcendentals=0
        ),
        name="attend_rows",
    )(place, queries, all_pairs, log_gate_cum, mix_weight, results)
    from_left = lax.ppermute(right, "tp", to_right)
    from_right = lax.ppermute(left, "tp", to_left)
    from_far = lax.ppermute(far, "tp", to_far)
    projected = (
        own.astype(jnp.float32)
        + from_left.astype(jnp.float32)
        + from_right.astype(jnp.float32)
        + from_far.astype(jnp.float32)
    )
    mix_result = rms_scale(projected, mix_gain).astype(jnp.bfloat16)
    moe_result = pl.pallas_call(
        combine_kernel,
        out_shape=jax.ShapeDtypeStruct((rows_here, width), jnp.bfloat16),
        in_specs=[VMEM, VMEM, VMEM],
        out_specs=VMEM,
        scratch_shapes=[pltpu.VMEM((LANES // 128, ep_count * groups, 128), jnp.float32)],
        name="combine_rows",
    )(lane_routes, lane_weight, returned)
    return (mix_result, moe_result)


def solution(mesh):
    in_specs = (
        P("ep", "tp"),
        P("ep", "tp"),
        P("tp", None),
        P("tp", None),
        P(),
        P(("ep", "tp"), None),
        P(),
        P(("ep", "tp"), None),
        P(("ep", "tp"), None),
        P("ep", None, "tp"),
        P("ep", None, "tp"),
        P("ep", "tp", None),
    )
    out_specs = (P(("ep", "tp"), None), P(("ep", "tp"), None))
    return jax.shard_map(body, mesh=mesh, in_specs=in_specs, out_specs=out_specs, check_vma=False)
```

time: 436 us -> 221 us (0.51)
  waiting for transfers between devices: 248 us -> 124 us
  local copies, waits for them, and re-layouts: 87.9 us -> 3.98 us
  Pallas kernels: 0 us -> 34.8 us
  matrix products: 17.1 us -> 0 us
  other arithmetic: 17.9 us -> 3.69 us
  starting transfers between devices: 46 us -> 39.5 us
    all_to_all x3 -> x2, waiting for transfers between devices: 196 us -> 30.6 us  [the longest x1 30.5 us: body(): returned = lax.all_to_all(results, 'ep', 0, 0, tiled=True)]
    ppermute x0 -> x13, waiting for transfers between devices: none -> 93 us  [the longest x1 20.8 us: body(): gate_f = lax.ppermute(gate_r, 'tp', to_right)]
    dynamic_slice x65 -> x0, local copies, waits for them, and re-layouts: 52.7 us -> none  [the longest x32 29.5 us: one_block(): lax.dynamic_slice_in_dim(piece, turn_index * block_rows, block_rows, 0)]
    all_gather x3 -> x1, waiting for transfers between devices: 51.2 us -> 0.01 us  [body(): all_pairs = lax.all_gather(keys_values, 'ep', axis=0, tiled=True)]
    pallas_call x0 -> x5, Pallas kernels: none -> 34.8 us  [the longest x1 10.3 us: body(): pl.pallas_call(down_kernel, out_shape=exchange_shape, in_specs=[VMEM] + [...]
    all_to_all x3 -> x2, starting transfers between devices: 45.9 us -> 22.2 us  [the longest x1 11.9 us: body(): received = lax.all_to_all(outgoing, 'ep', 0, 0, tiled=True)]
    ppermute x0 -> x13, starting transfers between devices: none -> 17.2 us  [the longest x1 2.15 us: body(): from_far = lax.ppermute(far, 'tp', to_far)]
    dot_general x11 -> x0, matrix products: 17.1 us -> none  [the longest x4 5.83 us: body(): jnp.dot(columns, add_piece[part_index * shard_rows:(part_index + 1) * sha...]
  transfers between devices with their start and end apart: 6 -> 16, of which waited for: 4 -> 9; matrix products, arithmetic and copies ran while one was open for 23% -> 2% of each run, Pallas kernels for 0% -> 14%
where the time goes in v1:
time: 221 us; the launch traced here: 220 us
  waiting for transfers between devices  124 us (56%)
  starting transfers between devices  39.5 us (18%)
  Pallas kernels  34.8 us (16%)
  between operations  14.2 us (6%)
  local copies, waits for them, and re-layouts  3.98 us (2%)
  other arithmetic  3.69 us (2%)
    all_to_all x1, waiting for transfers between devices, body(): returned = lax.all_to_all(results, 'ep', 0, 0, tiled=True)  30.5 us
    ppermute x1, waiting for transfers between devices, body(): gate_f = lax.ppermute(gate_r, 'tp', to_right)  20.8 us
    ppermute x1, waiting for transfers between devices, body(): gate_r = lax.ppermute(gate, 'tp', to_right)  20.6 us
    ppermute x1, waiting for transfers between devices, body(): down_r = lax.ppermute(down, 'tp', to_right)  19.6 us
    ppermute x1, waiting for transfers between devices, body(): up_r = lax.ppermute(up, 'tp', to_right)  19.6 us
    all_to_all x1, starting transfers between devices, body(): received = lax.all_to_all(outgoing, 'ep', 0, 0, tiled=True)  11.9 us
    all_to_all x1, starting transfers between devices, body(): returned = lax.all_to_all(results, 'ep', 0, 0, tiled=True)  10.3 us
    pallas_call x1, Pallas kernels, body(): pl.pallas_call(down_kernel, out_shape=exchange_shape, in_specs=[VMEM] + [...  10.3 us
  transfers between devices with their start and end apart: 16, of which 9 were waited for; matrix products, arithmetic and copies ran while one was open for 2% of the time, Pallas kernels for 14%

profile of v1, /device:TPU:8, one launch (start us, length us, event | category | flops | bytes accessed | tf_op | source)
XLA Modules:
  0.0 220.4 jit_solution(17514214520561783947)
XLA Ops:
  7.9 3.6 %dispatch_rows.1 = bf16[64,72,256]{2,1,0:T(8,128)(2,1)} custom-call(s32[2,192]{1,0:T(2,128)} %bitcast.8, bf16[192,2048]{1,0:T(8,128)(2,1)} %tokens_ref.1), custom_call_target="tpu_custom_call" | custom-call | tf_op jit(solution)/shard_map/dispatch_rows/pallas_call | solution.py:321
  11.5 11.9 %all-to-all-start = ((bf16[64,72,256]{2,1,0:T(8,128)(2,1)}), bf16[64,72,256]{2,1,0:T(8,128)(2,1)S(1)}, u32[]{:S(2)}, u32[]{:S(2)}) async-start(bf16[64,72,256]{2,1,0:T(8,128)(2,1)} %dispatch_rows.1), calls=%async_computation | async-start | bytes 4718592 | tf_op jit(solution)/shard_map/all_to_all | solution.py:329
  23.5 1.7 collective-permute-start
  25.6 1.6 collective-permute-start.6
  27.6 1.6 collective-permute-start.1
  29.2 20.6 %collective-permute-done.g1 = bf16[2048,256]{1,0:T(8,128)(2,1)S(1)} collective-permute-done((bf16[2048,256]{1,0:T(8,128)(2,1)}, bf16[2048,256]{1,0:T(8,128)(2,1)S(1)}, u32[]{:S(2)}, u32[]{:S(2)}) %collective-permute-start) | collective-permute-done | bytes 1048608 | tf_op jit(solution)/shard_map/ppermute | solution.py:307
  49.8 1.7 collective-permute-start.2
  52.7 19.6 %collective-permute-done.6.d1 = bf16[256,2048]{1,0:T(8,128)(2,1)S(1)} collective-permute-done((bf16[256,2048]{1,0:T(8,128)(2,1)}, bf16[256,2048]{1,0:T(8,128)(2,1)S(1)}, u32[]{:S(2)}, u32[]{:S(2)}) %collective-permute-start.6) | collective-permute-done | bytes 1048608 | tf_op jit(solution)/shard_map/ppermute | solution.py:313
  72.3 1.7 collective-permute-start.5
  75.2 19.6 %collective-permute-done.1.u1 = bf16[2048,256]{1,0:T(8,128)(2,1)S(1)} collective-permute-done((bf16[2048,256]{1,0:T(8,128)(2,1)}, bf16[2048,256]{1,0:T(8,128)(2,1)S(1)}, u32[]{:S(2)}, u32[]{:S(2)}) %collective-permute-start.1) | collective-permute-done | bytes 1048608 | tf_op jit(solution)/shard_map/ppermute | solution.py:309
  94.7 1.7 collective-permute-start.9
  96.4 20.8 %collective-permute-done.4.g3 = bf16[2048,256]{1,0:T(8,128)(2,1)S(1)} collective-permute-done((bf16[2048,256]{1,0:T(8,128)(2,1)S(1)}, bf16[2048,256]{1,0:T(8,128)(2,1)S(1)}, u32[]{:S(2)}, u32[]{:S(2)}) %collective-permute-start.4) | collective-permute-done | bytes 1048608 | tf_op jit(solution)/shard_map/ppermute | solution.py:311
  118.9 1.5 copy-done.1
  120.4 9.9 %hidden_rows.1.hidden_ref = bf16[576,1024]{1,0:T(8,128)(2,1)} custom-call(bf16[64,72,256]{2,1,0:T(8,128)(2,1)} %copy-done.1, f32[1,2048]{1,0:T(1,128)} %bitcast.11, bf16[2048,256]{1,0:T(8,128)(2,1)} %bitcast.4.g0, bf16[2048,256]{1,0:T(8,128)(2,1)} %bitcast.5.u0, bf16[2048,256]{1,0:T(8,128)(2,1)} %copy-done.5, bf16[2048,256]{1,0:T(8,128)(2,1)} %copy-done.7, ...), custom_call_target="tpu_custom_call" | custom-call | flops 4831838208 | bytes 12000000 | tf_op jit(solution)/shard_map/hidden_rows/pallas_call | solution.py:330
  130.3 10.3 %down_rows.1.after_ref = bf16[64,72,256]{2,1,0:T(8,128)(2,1)} custom-call(bf16[576,1024]{1,0:T(8,128)(2,1)} %hidden_rows.1.hidden_ref, bf16[256,2048]{1,0:T(8,128)(2,1)} %bitcast.6.d0, bf16[256,2048]{1,0:T(8,128)(2,1)} %copy-done.2, bf16[256,2048]{1,0:T(8,128)(2,1)} %copy-done.3, bf16[128,2048]{1,0:T(8,128)(2,1)} %collective-permute-done.8.d3a, ...), custom_call_target="tpu_custom_call" | custom-call | flops 2415919104 | bytes 8000000 | tf_op jit(solution)/shard_map/down_rows/pallas_call | solution.py:352
  140.6 10.3 %all-to-all-start.1 = ((bf16[64,72,256]{2,1,0:T(8,128)(2,1)}), bf16[64,72,256]{2,1,0:T(8,128)(2,1)S(1)}, u32[]{:S(2)}, u32[]{:S(2)}) async-start(bf16[64,72,256]{2,1,0:T(8,128)(2,1)} %down_rows.1.after_ref), calls=%async_computation.1 | async-start | bytes 4718592 | tf_op jit(solution)/shard_map/all_to_all | solution.py:369
  151.6 6.7 %attend_rows.1 = (bf16[64,2048]{1,0:T(8,128)(2,1)}, bf16[64,2048]{1,0:T(8,128)(2,1)}, bf16[64,2048]{1,0:T(8,128)(2,1)}, bf16[64,2048]{1,0:T(8,128)(2,1)}) custom-call(s32[2]{0:T(128)} %pad_add_fusion.place_ref, bf16[256,256]{1,0:T(8,128)(2,1)} %queries_ref.1, bf16[16384,128]{1,0:T(8,128)(2,1)} %all-gather.2.cloned.1.call-done.keys_ref, f32[4,16384]{1,0:T(4,128)} %gate_ref.1, ...), custom_call_target="tpu_custom_call" | custom-call | flops 30000001024 | bytes 5000000 | tf_op jit(solution)/shard_map/attend_rows/pallas_call | solution.py:374
  160.3 2.2 collective-permute-start.12
  162.5 5.2 %collective-permute-done.10 = bf16[64,2048]{1,0:T(8,128)(2,1)S(1)} collective-permute-done((bf16[64,2048]{1,0:T(8,128)(2,1)}, bf16[64,2048]{1,0:T(8,128)(2,1)S(1)}, u32[]{:S(2)}, u32[]{:S(2)}) %collective-permute-start.10) | collective-permute-done | bytes 262176 | tf_op jit(solution)/shard_map/ppermute | solution.py:390
  168.1 6.2 %collective-permute-done.12 = bf16[64,2048]{1,0:T(8,128)(2,1)S(1)} collective-permute-done((bf16[64,2048]{1,0:T(8,128)(2,1)}, bf16[64,2048]{1,0:T(8,128)(2,1)S(1)}, u32[]{:S(2)}, u32[]{:S(2)}) %collective-permute-start.12) | collective-permute-done | bytes 262176 | tf_op jit(solution)/shard_map/ppermute | solution.py:392
  175.5 1.8 multiply_convert_fusion
  177.3 30.5 %all-to-all-done.1.returned_ref = bf16[64,72,256]{2,1,0:T(8,128)(2,1)S(1)} async-done(((bf16[64,72,256]{2,1,0:T(8,128)(2,1)}), bf16[64,72,256]{2,1,0:T(8,128)(2,1)S(1)}, u32[]{:S(2)}, u32[]{:S(2)}) %all-to-all-start.1) | async-done | bytes 2359328 | tf_op jit(solution)/shard_map/all_to_all | solution.py:369
  207.9 1.4 copy-done
  209.3 4.2 %combine_rows.1 = bf16[192,2048]{1,0:T(8,128)(2,1)} custom-call(s32[2,192]{1,0:T(2,128)} %bitcast.9, f32[2,192]{1,0:T(2,128)} %bitcast.10, bf16[64,72,256]{2,1,0:T(8,128)(2,1)} %copy-done), custom_call_target="tpu_custom_call" | custom-call | tf_op jit(solution)/shard_map/combine_rows/pallas_call | solution.py:400
  (40 shorter events, 10.0 us)
Async XLA Ops:
  7.2 144.4 %all-gather.2.cloned.1.call-start = ((), (), s32[]{:S(2)}) async-start(), calls=%async_computation.2 | async-start | bytes 4259840 | tf_op jit(solution)/shard_map/all_gather | solution.py:318
  11.5 107.4 %all-to-all-start = ((bf16[64,72,256]{2,1,0:T(8,128)(2,1)}), bf16[64,72,256]{2,1,0:T(8,128)(2,1)S(1)}, u32[]{:S(2)}, u32[]{:S(2)}) async-start(bf16[64,72,256]{2,1,0:T(8,128)(2,1)} %dispatch_rows.1), calls=%async_computation | async-start | bytes 4718592 | tf_op jit(solution)/shard_map/all_to_all | solution.py:329
  23.5 26.3 %collective-permute-start = (bf16[2048,256]{1,0:T(8,128)(2,1)}, bf16[2048,256]{1,0:T(8,128)(2,1)S(1)}, u32[]{:S(2)}, u32[]{:S(2)}) collective-permute-start(bf16[2048,256]{1,0:T(8,128)(2,1)} %bitcast.4.g0), channel_id=1, source_target_pairs={{0,1},{1,2},{2,3},{3,0},{4,5},{5,6},{6,7},{7,4},{8,9},{9,10},{10,1... | collective-permute-start | bytes 3145736 | tf_op jit(solution)/shard_map/ppermute | solution.py:307
  25.1 26.3 %collective-permute-start.3 = (bf16[2048,256]{1,0:T(8,128)(2,1)}, bf16[2048,256]{1,0:T(8,128)(2,1)S(1)}, u32[]{:S(2)}, u32[]{:S(2)}) collective-permute-start(bf16[2048,256]{1,0:T(8,128)(2,1)} %bitcast.5.u0), channel_id=1, source_target_pairs={{0,3},{1,0},{2,1},{3,2},{4,7},{5,4},{6,5},{7,6},{8,11},{9,8},{10,9... | collective-permute-start | bytes 3145736 | tf_op jit(solution)/shard_map/ppermute | solution.py:308
  25.6 46.7 %collective-permute-start.6 = (bf16[256,2048]{1,0:T(8,128)(2,1)}, bf16[256,2048]{1,0:T(8,128)(2,1)S(1)}, u32[]{:S(2)}, u32[]{:S(2)}) collective-permute-start(bf16[256,2048]{1,0:T(8,128)(2,1)} %bitcast.6.d0), channel_id=1, source_target_pairs={{0,1},{1,2},{2,3},{3,0},{4,5},{5,6},{6,7},{7,4},{8,9},{9,10},{10,1... | collective-permute-start | bytes 3145736 | tf_op jit(solution)/shard_map/ppermute | solution.py:313
  27.2 46.8 %collective-permute-start.7 = (bf16[256,2048]{1,0:T(8,128)(2,1)}, bf16[256,2048]{1,0:T(8,128)(2,1)S(1)}, u32[]{:S(2)}, u32[]{:S(2)}) collective-permute-start(bf16[256,2048]{1,0:T(8,128)(2,1)} %bitcast.6.d0), channel_id=1, source_target_pairs={{0,3},{1,0},{2,1},{3,2},{4,7},{5,4},{6,5},{7,6},{8,11},{9,8},{10,9... | collective-permute-start | bytes 3145736 | tf_op jit(solution)/shard_map/ppermute | solution.py:314
  27.6 67.1 %collective-permute-start.1 = (bf16[2048,256]{1,0:T(8,128)(2,1)}, bf16[2048,256]{1,0:T(8,128)(2,1)S(1)}, u32[]{:S(2)}, u32[]{:S(2)}) collective-permute-start(bf16[2048,256]{1,0:T(8,128)(2,1)} %bitcast.5.u0), channel_id=1, source_target_pairs={{0,1},{1,2},{2,3},{3,0},{4,5},{5,6},{6,7},{7,4},{8,9},{9,10},{10,1... | collective-permute-start | bytes 3145736 | tf_op jit(solution)/shard_map/ppermute | solution.py:309
  49.8 67.4 %copy-start.5 = (bf16[2048,256]{1,0:T(8,128)(2,1)}, bf16[2048,256]{1,0:T(8,128)(2,1)S(1)}, u32[]{:S(2)}) copy-start(bf16[2048,256]{1,0:T(8,128)(2,1)S(1)} %collective-permute-done.g1) | copy-start | bytes 3145732
  49.8 46.6 %collective-permute-start.2 = (bf16[2048,256]{1,0:T(8,128)(2,1)}, bf16[2048,256]{1,0:T(8,128)(2,1)S(1)}, u32[]{:S(2)}, u32[]{:S(2)}) collective-permute-start(bf16[2048,256]{1,0:T(8,128)(2,1)} %bitcast.4.g0), channel_id=1, source_target_pairs={{0,3},{1,0},{2,1},{3,2},{4,7},{5,4},{6,5},{7,6},{8,11},{9,8},{10,9... | collective-permute-start | bytes 3145736 | tf_op jit(solution)/shard_map/ppermute | solution.py:310
  51.5 65.8 %copy-start.6 = (bf16[2048,256]{1,0:T(8,128)(2,1)}, bf16[2048,256]{1,0:T(8,128)(2,1)S(1)}, u32[]{:S(2)}) copy-start(bf16[2048,256]{1,0:T(8,128)(2,1)S(1)} %collective-permute-done.3.u2) | copy-start | bytes 3145732
  51.5 65.7 %collective-permute-start.4 = (bf16[2048,256]{1,0:T(8,128)(2,1)S(1)}, bf16[2048,256]{1,0:T(8,128)(2,1)S(1)}, u32[]{:S(2)}, u32[]{:S(2)}) collective-permute-start(bf16[2048,256]{1,0:T(8,128)(2,1)S(1)} %collective-permute-done.g1), channel_id=1, source_target_pairs={{0,1},{1,2},{2,3},{3,0},{4,5},{5,6},{6,7},{7,4},{8,9},{9,10},{10,1... | collective-permute-start | bytes 3145736 | tf_op jit(solution)/shard_map/ppermute | solution.py:311
  72.3 44.9 %copy-start.2 = (bf16[256,2048]{1,0:T(8,128)(2,1)}, bf16[256,2048]{1,0:T(8,128)(2,1)S(1)}, u32[]{:S(2)}) copy-start(bf16[256,2048]{1,0:T(8,128)(2,1)S(1)} %collective-permute-done.6.d1) | copy-start | bytes 3145732
  72.3 46.6 %collective-permute-start.5 = (bf16[2048,256]{1,0:T(8,128)(2,1)S(1)}, bf16[2048,256]{1,0:T(8,128)(2,1)}, u32[]{:S(2)}, u32[]{:S(2)}) collective-permute-start(bf16[2048,256]{1,0:T(8,128)(2,1)S(1)} %collective-permute-done.3.u2), channel_id=1, source_target_pairs={{0,3},{1,0},{2,1},{3,2},{4,7},{5,4},{6,5},{7,6},{8,11},{9,8},{10,9... | collective-permute-start | bytes 3145736 | tf_op jit(solution)/shard_map/ppermute | solution.py:312
  74.0 43.2 %copy-start.3 = (bf16[256,2048]{1,0:T(8,128)(2,1)}, bf16[256,2048]{1,0:T(8,128)(2,1)S(1)}, u32[]{:S(2)}) copy-start(bf16[256,2048]{1,0:T(8,128)(2,1)S(1)} %collective-permute-done.7.d2) | copy-start | bytes 3145732
  74.0 56.3 %collective-permute-start.8 = (bf16[128,2048]{1,0:T(8,128)(2,1)S(1)}, bf16[128,2048]{1,0:T(8,128)(2,1)}, u32[]{:S(2)}, u32[]{:S(2)}) collective-permute-start(bf16[128,2048]{1,0:T(8,128)(2,1)S(1)} %slice.8), channel_id=1, source_target_pairs={{0,1},{1,2},{2,3},{3,0},{4,5},{5,6},{6,7},{7,4},{8,9},{9,10},{10,1... | collective-permute-start | bytes 1572872 | tf_op jit(solution)/shard_map/ppermute | solution.py:315
  94.7 22.5 %copy-start.7 = (bf16[2048,256]{1,0:T(8,128)(2,1)}, bf16[2048,256]{1,0:T(8,128)(2,1)S(1)}, u32[]{:S(2)}) copy-start(bf16[2048,256]{1,0:T(8,128)(2,1)S(1)} %collective-permute-done.1.u1) | copy-start | bytes 3145732
  94.7 35.6 %collective-permute-start.9 = (bf16[128,2048]{1,0:T(8,128)(2,1)S(1)}, bf16[128,2048]{1,0:T(8,128)(2,1)}, u32[]{:S(2)}, u32[]{:S(2)}) collective-permute-start(bf16[128,2048]{1,0:T(8,128)(2,1)S(1)} %slice.9), channel_id=1, source_target_pairs={{0,3},{1,0},{2,1},{3,2},{4,7},{5,4},{6,5},{7,6},{8,11},{9,8},{10,9... | collective-permute-start | bytes 1572872 | tf_op jit(solution)/shard_map/ppermute | solution.py:316
  96.4 20.8 %copy-start.8 = (bf16[2048,256]{1,0:T(8,128)(2,1)}, bf16[2048,256]{1,0:T(8,128)(2,1)S(1)}, u32[]{:S(2)}) copy-start(bf16[2048,256]{1,0:T(8,128)(2,1)S(1)} %collective-permute-done.2.g2) | copy-start | bytes 3145732
  118.9 1.5 copy-start.1
  140.6 67.3 %all-to-all-start.1 = ((bf16[64,72,256]{2,1,0:T(8,128)(2,1)}), bf16[64,72,256]{2,1,0:T(8,128)(2,1)S(1)}, u32[]{:S(2)}, u32[]{:S(2)}) async-start(bf16[64,72,256]{2,1,0:T(8,128)(2,1)} %down_rows.1.after_ref), calls=%async_computation.1 | async-start | bytes 4718592 | tf_op jit(solution)/shard_map/all_to_all | solution.py:369
  151.6 23.9 %copy-start.4 = (f32[2048]{0:T(1024)S(1)}, f32[2048]{0:T(1024)}, u32[]{:S(2)}) copy-start(f32[2048]{0:T(1024)} %param.16) | copy-start | bytes 24580
  158.3 9.4 %collective-permute-start.10 = (bf16[64,2048]{1,0:T(8,128)(2,1)}, bf16[64,2048]{1,0:T(8,128)(2,1)S(1)}, u32[]{:S(2)}, u32[]{:S(2)}) collective-permute-start(bf16[64,2048]{1,0:T(8,128)(2,1)} %get-tuple-element.7), channel_id=1, source_target_pairs={{0,1},{1,2},{2,3},{3,0},{4,5},{5,6},{6,7},{7,4},{8,9},{9,10},{10,1... | collective-permute-start | bytes 786440 | tf_op jit(solution)/shard_map/ppermute | solution.py:390
  159.6 8.5 %collective-permute-start.11 = (bf16[64,2048]{1,0:T(8,128)(2,1)}, bf16[64,2048]{1,0:T(8,128)(2,1)S(1)}, u32[]{:S(2)}, u32[]{:S(2)}) collective-permute-start(bf16[64,2048]{1,0:T(8,128)(2,1)} %get-tuple-element.8), channel_id=1, source_target_pairs={{0,3},{1,0},{2,1},{3,2},{4,7},{5,4},{6,5},{7,6},{8,11},{9,8},{10,9... | collective-permute-start | bytes 786440 | tf_op jit(solution)/shard_map/ppermute | solution.py:391
  160.3 13.9 %collective-permute-start.12 = (bf16[64,2048]{1,0:T(8,128)(2,1)}, bf16[64,2048]{1,0:T(8,128)(2,1)S(1)}, u32[]{:S(2)}, u32[]{:S(2)}) collective-permute-start(bf16[64,2048]{1,0:T(8,128)(2,1)} %get-tuple-element.9), channel_id=1, source_target_pairs={{0,2},{1,3},{2,0},{3,1},{4,6},{5,7},{6,4},{7,5},{8,10},{9,11},{10,... | collective-permute-start | bytes 786440 | tf_op jit(solution)/shard_map/ppermute | solution.py:392
  (2 other events, 2.4 us)
Sparse Core Ops, SparseCore 0:
  10.7 87.9 all-gather.1

commit v2 on v1

--- a/solution.py
+++ b/solution.py
@@ -10,7 +10,6 @@
 EPSILON = 1e-06
 NEGATIVE = -1e30
 LANES = 256
-KEY_BLOCK = 1024
 LOG2E = 1.4426950408889634
 
 
@@ -72,24 +71,22 @@
     out_ref[:, 8 * groups :, :] = whole.reshape(experts, groups, LANES).astype(jnp.bfloat16)
 
 
-def hidden_kernel(
-    received_ref, gain_ref,
-    g0, u0, g1, u1, g2, u2, g3, u3,
-    hidden_ref,
-    gate_buf, up_buf, tokens_ref, ninth_ref, sems,
+def silu_product(tokens, gate, up):
+    gated = jnp.dot(tokens, gate, preferred_element_type=jnp.float32)
+    lifted = jnp.dot(tokens, up, preferred_element_type=jnp.float32)
+    return (gated / (1.0 + jnp.exp(-gated)) * lifted).astype(jnp.bfloat16)
+
+
+def near_kernel(
+    received_ref, gain_ref, g0, u0, g1, u1, g2, u2,
+    hidden_ref, tokens_ref,
+    ninth_ref,
 ):
     sources = received_ref.shape[0]
     groups = received_ref.shape[1] // 9
     width = groups * LANES
     eights = sources * 8
     ff = g0.shape[1]
-    copies = []
-    for n, (g, u) in enumerate(((g0, u0), (g1, u1), (g2, u2), (g3, u3))):
-        copies.append(pltpu.make_async_copy(g, gate_buf.at[n], sems.at[2 * n]))
-        copies.append(pltpu.make_async_copy(u, up_buf.at[n], sems.at[2 * n + 1]))
-    for c in copies:
-        c.start()
-
     ninth = received_ref[:, 8 * groups :, :].astype(jnp.float32).reshape(sources * groups, LANES)
     for h in range(LANES // 128):
         ninth_ref[h] = ninth[:, h * 128 : (h + 1) * 128]
@@ -120,95 +117,97 @@
         tokens_ref[eights:, g * LANES : (g + 1) * LANES] = (
             ninth_rows(g) * scale9 * gain
         ).astype(jnp.bfloat16)
-
-    for n in range(4):
-        copies[2 * n].wait()
-        copies[2 * n + 1].wait()
-        gated = jnp.dot(tokens_ref[...], gate_buf[n], preferred_element_type=jnp.float32)
-        lifted = jnp.dot(tokens_ref[...], up_buf[n], preferred_element_type=jnp.float32)
-        hidden_ref[:, n * ff : (n + 1) * ff] = (
-            gated / (1.0 + jnp.exp(-gated)) * lifted
-        ).astype(jnp.bfloat16)
-
-
-def down_kernel(hidden_ref, d0, d1, d2, d3a, d3b, out_ref, down_buf, ninth_ref, sems):
+    for n, (gate, up) in enumerate(((g0, u0), (g1, u1), (g2, u2))):
+        hidden_ref[:, n * ff : (n + 1) * ff] = silu_product(tokens_ref[...], gate[...], up[...])
+
+
+def far_kernel(tokens_ref, gate, up, near_ref, d0, d1, d2, hidden_ref, sum_ref):
+    hidden_ref[...] = silu_product(tokens_ref[...], gate[...], up[...])
+    for g in range(d0.shape[1] // LANES):
+        columns = slice(g * LANES, (g + 1) * LANES)
+        down = jnp.concatenate([d[:, columns] for d in (d0, d1, d2)], axis=0)
+        sum_ref[:, columns] = jnp.dot(near_ref[...], down, preferred_element_type=jnp.float32)
+
+
+def down_kernel(sum_ref, far_ref, d3a, d3b, out_ref, built_ref, ninth_ref, sems):
     sources = out_ref.shape[0]
     groups = out_ref.shape[1] // 9
     eights = sources * 8
-    ff = d0.shape[0]
-    half = d3a.shape[0]
-    pieces = ((d0, 0, ff), (d1, ff, ff), (d2, 2 * ff, ff), (d3a, 3 * ff, half), (d3b, 3 * ff + half, half))
-    copies = []
+    leaving = []
+
+    def leave(part, size):
+        rows = pl.ds(part * 8, size)
+        copy = pltpu.make_async_copy(
+            built_ref.at[:, rows, :], out_ref.at[:, rows, :], sems.at[part]
+        )
+        copy.start()
+        leaving.append(copy)
+
     for g in range(groups):
-        columns = pl.ds(g * LANES, LANES)
-        copies.append(
-            [
-                pltpu.make_async_copy(
-                    d.at[:, columns], down_buf.at[g, pl.ds(at, size), :], sems.at[5 * g + n]
-                )
-                for n, (d, at, size) in enumerate(pieces)
-            ]
+        columns = slice(g * LANES, (g + 1) * LANES)
+        result = sum_ref[:, columns] + jnp.dot(
+            far_ref[...],
+            jnp.concatenate([d3a[:, columns], d3b[:, columns]], axis=0),
+            preferred_element_type=jnp.float32,
         )
-    for group in copies:
-        for c in group:
-            c.start()
-    for g in range(groups):
-        for c in copies[g]:
-            c.wait()
-        result = jnp.dot(hidden_ref[...], down_buf[g], preferred_element_type=jnp.float32)
-        out_ref[:, g * 8 : (g + 1) * 8, :] = (
+        built_ref[:, g * 8 : (g + 1) * 8, :] = (
             result[:eights].reshape(sources, 8, LANES).astype(jnp.bfloat16)
         )
+        leave(g, 8)
         for h in range(LANES // 128):
             ninth_ref[h, pl.ds(g, sources, stride=groups), :] = result[
                 eights:, h * 128 : (h + 1) * 128
             ]
     whole = jnp.concatenate([ninth_ref[h] for h in range(LANES // 128)], axis=1)
-    out_ref[:, 8 * groups :, :] = whole.reshape(sources, groups, LANES).astype(jnp.bfloat16)
+    built_ref[:, 8 * groups :, :] = whole.reshape(sources, groups, LANES).astype(jnp.bfloat16)
+    leave(groups, groups)
+    for copy in leaving:
+        copy.wait()
+
+
+def stack_kernel(*refs):
+    rows = refs[0].shape[0]
+    for n, ref in enumerate(refs[:-1]):
+        refs[-1][n * rows : (n + 1) * rows, :] = ref[...]
 
 
 def attention_kernel(
-    place_ref, queries_ref, keys_ref, gate_ref, mix_ref, after_ref,
+    place_ref, queries_ref, gate_ref, mix_ref,
+    k0, k1, k2, k3, k4, k5, k6, k7,
     own_ref, right_ref, left_ref, far_ref,
     scaled_ref, sums_ref, top_ref, mixed_ref,
 ):
     rows = queries_ref.shape[0]
     heads = queries_ref.shape[1] // HEAD
-    block = min(KEY_BLOCK, keys_ref.shape[0])
     quarter = own_ref.shape[0]
-    first_row = place_ref[0] * rows
+    plane, column, core = place_ref[0], place_ref[1], place_ref[2]
+    sources = ((k0, 0, 0), (k1, 1, 0), (k2, 3, 0), (k3, 2, 0), (k4, 0, 1), (k5, 1, 1), (k6, 3, 1), (k7, 2, 1))
     for h in range(heads):
         part = queries_ref[:, h * HEAD : (h + 1) * HEAD].astype(jnp.float32) * HEAD ** (-0.5)
         scaled_ref[h] = jnp.concatenate([part, jnp.zeros_like(part)], axis=1).astype(jnp.bfloat16)
     sums_ref[...] = jnp.zeros_like(sums_ref)
     top_ref[...] = jnp.full_like(top_ref, NEGATIVE)
-    value_lane = lax.broadcasted_iota(jnp.int32, (block, 2 * HEAD), 1) >= HEAD
-
-    def fold(start, masked):
-        pairs = keys_ref[pl.ds(start, block), :]
-        values = jnp.where(value_lane, pairs.astype(jnp.float32), 1.0).astype(jnp.bfloat16)
-        if masked:
-            query_pos = first_row + lax.broadcasted_iota(jnp.int32, (rows, block), 0)
-            key_pos = start + lax.broadcasted_iota(jnp.int32, (rows, block), 1)
-            causal = key_pos <= query_pos
+    own_index = plane * 8 + column * 2 + core
+
+    def fold(pairs, gates, causal):
+        lane = lax.broadcasted_iota(jnp.int32, pairs.shape, 1)
+        values = jnp.where(lane >= HEAD, pairs.astype(jnp.float32), 1.0).astype(jnp.bfloat16)
         scores = [
             lax.dot_general(
                 scaled_ref[h], pairs, (((1,), (1,)), ((), ())), preferred_element_type=jnp.float32
             )
             * LOG2E
-            - gate_ref[h : h + 1, pl.ds(start, block)] * LOG2E
+            - gates[h : h + 1, :] * LOG2E
             for h in range(heads)
         ]
         folded = []
         for h in range(heads):
             score = scores[h]
-            if masked:
+            if causal is not None:
                 score = jnp.where(causal, score, NEGATIVE)
             old_top = top_ref[h][:, 0:1]
             new_top = jnp.maximum(old_top, jnp.max(score, axis=1, keepdims=True))
             weight = jnp.exp2(score - new_top)
-            if masked:
-                weight = jnp.where(causal, weight, 0.0)
             top_ref[h] = jnp.broadcast_to(new_top, top_ref.shape[1:])
             folded.append((weight.astype(jnp.bfloat16), jnp.exp2(old_top - new_top)))
         for h in range(heads):
@@ -217,14 +216,26 @@
                 weight, values, preferred_element_type=jnp.float32
             )
 
-    whole_blocks = first_row // block
-
-    def step(i, carry):
-        fold(pl.multiple_of(i * block, block), False)
+    fold(
+        k0[:rows, :],
+        gate_ref[:, pl.ds(pl.multiple_of(own_index * rows, rows), rows)],
+        lax.broadcasted_iota(jnp.int32, (rows, rows), 1)
+        <= lax.broadcasted_iota(jnp.int32, (rows, rows), 0),
+    )
+
+    def step(back, carry):
+        at = pl.multiple_of(back * rows, rows)
+        for group in range(2):
+            pairs, gates = [], []
+            for keys, across, other in sources[group * 4 : (group + 1) * 4]:
+                index = (plane - back) * 8 + ((column + 4 - across) % 4) * 2 + (core + other) % 2
+                gate = gate_ref[:, pl.ds(pl.multiple_of(index * rows, rows), rows)]
+                pairs.append(keys[pl.ds(at, rows), :])
+                gates.append(jnp.where(index < own_index, gate, -NEGATIVE))
+            fold(jnp.concatenate(pairs, axis=0), jnp.concatenate(gates, axis=1), None)
         return carry
 
-    lax.fori_loop(0, whole_blocks, step, 0)
-    fold(pl.multiple_of(whole_blocks * block, block), True)
+    lax.fori_loop(0, plane + 1, step, 0)
     mixed = []
     for h in range(heads):
         total = sums_ref[h]
@@ -232,7 +243,7 @@
     mixed_ref[...] = jnp.concatenate(mixed, axis=1).astype(jnp.bfloat16)
     parts = 4
     for shift, out_ref in ((0, own_ref), (1, right_ref), (3, left_ref), (2, far_ref)):
-        at = pl.multiple_of(((place_ref[1] + shift) % parts) * quarter, quarter)
+        at = pl.multiple_of(((place_ref[3] + shift) % parts) * quarter, quarter)
         out_ref[...] = jnp.dot(
             mixed_ref[pl.ds(at, quarter), :], mix_ref[...], preferred_element_type=jnp.float32
         ).astype(jnp.bfloat16)
@@ -274,7 +285,24 @@
 
 VMEM = pl.BlockSpec(memory_space=pltpu.VMEM)
 SMEM = pl.BlockSpec(memory_space=pltpu.SMEM)
-ANY = pl.BlockSpec(memory_space=pl.ANY)
+HBM = pl.BlockSpec(memory_space=pltpu.HBM)
+
+
+def on_chip(array):
+    return pltpu.with_memory_space_constraint(array, pltpu.VMEM)
+
+
+def kept_on_chip(shape):
+    return jax.ShapeDtypeStruct(shape, jnp.bfloat16)
+
+
+def shift_pairs(down, across, other):
+    return [
+        (z * 8 + x * 2 + c, (z + down) % 8 * 8 + (x + across) % 4 * 2 + (c + other) % 2)
+        for z in range(8)
+        for x in range(4)
+        for c in range(2)
+    ]
 
 
 def body(
@@ -293,7 +321,10 @@
 ):
     ep_count = lax.axis_size("ep")
     tp_count = lax.axis_size("tp")
-    place = jnp.stack([lax.axis_index("ep"), lax.axis_index("tp")]).astype(jnp.int32)
+    ep_index = lax.axis_index("ep")
+    place = jnp.stack(
+        [ep_index // 8, ep_index // 2 % 4, ep_index % 2, lax.axis_index("tp")]
+    ).astype(jnp.int32)
     to_right = [(i, (i + 1) % tp_count) for i in range(tp_count)]
     to_left = [(i, (i - 1) % tp_count) for i in range(tp_count)]
     to_far = [(i, (i + 2) % tp_count) for i in range(tp_count)]
@@ -308,64 +339,101 @@
     up_l = lax.ppermute(up, "tp", to_left)
     up_r = lax.ppermute(up, "tp", to_right)
     gate_l = lax.ppermute(gate, "tp", to_left)
+    down_r = lax.ppermute(down, "tp", to_right)
+    down_l = lax.ppermute(down, "tp", to_left)
     gate_f = lax.ppermute(gate_r, "tp", to_right)
     up_f = lax.ppermute(up_l, "tp", to_left)
-    down_r = lax.ppermute(down, "tp", to_right)
-    down_l = lax.ppermute(down, "tp", to_left)
     down_fa = lax.ppermute(down_r[: ff // 2], "tp", to_right)
     down_fb = lax.ppermute(down_l[ff // 2 :], "tp", to_left)
 
-    all_pairs = lax.all_gather(keys_values, "ep", axis=0, tiled=True)
-
-    exchange_shape = jax.ShapeDtypeStruct((ep_count, 9 * groups, LANES), jnp.bfloat16)
+    over_planes = [keys_values] + [
+        lax.ppermute(keys_values, "ep", shift_pairs(d, 0, 0)) for d in range(1, 8)
+    ]
+    column_keys = pl.pallas_call(
+        stack_kernel,
+        out_shape=jax.ShapeDtypeStruct(
+            (8 * keys_values.shape[0], keys_values.shape[1]), jnp.bfloat16
+        ),
+        in_specs=[VMEM] * 8,
+        out_specs=VMEM,
+        compiler_params=pltpu.CompilerParams(vmem_limit_bytes=8 * 2**20),
+        name="stack_rows",
+    )(*over_planes)
+    core_keys = [column_keys] + [
+        lax.ppermute(column_keys, "ep", shift_pairs(0, d, 0)) for d in (1, 3, 2)
+    ]
+    other_keys = [
+        lax.ppermute(k, "ep", shift_pairs(0, 0, 1)) for k in core_keys
+    ]
+
+    exchange_shape = kept_on_chip((ep_count, 9 * groups, LANES))
     outgoing = pl.pallas_call(
         dispatch_kernel,
         out_shape=exchange_shape,
         in_specs=[VMEM, VMEM],
         out_specs=VMEM,
         scratch_shapes=[pltpu.VMEM((LANES // 128, ep_count * groups, 128), jnp.float32)],
+        compiler_params=pltpu.CompilerParams(vmem_limit_bytes=16 * 2**20),
         name="dispatch_rows",
     )(lane_routes, moe_in)
     received = lax.all_to_all(outgoing, "ep", 0, 0, tiled=True)
-    hidden = pl.pallas_call(
-        hidden_kernel,
-        out_shape=jax.ShapeDtypeStruct((slot_rows, tp_count * ff), jnp.bfloat16),
-        in_specs=[VMEM, VMEM] + [ANY] * 8,
-        out_specs=VMEM,
+    near, normed = pl.pallas_call(
+        near_kernel,
+        out_shape=[
+            kept_on_chip((slot_rows, 3 * ff)),
+            kept_on_chip((slot_rows, width)),
+        ],
+        in_specs=[VMEM] * 8,
+        out_specs=[VMEM] * 2,
         scratch_shapes=[
-            pltpu.VMEM((tp_count, width, ff), jnp.bfloat16),
-            pltpu.VMEM((tp_count, width, ff), jnp.bfloat16),
-            pltpu.VMEM((slot_rows, width), jnp.bfloat16),
             pltpu.VMEM((LANES // 128, ep_count * groups, 128), jnp.float32),
-            pltpu.SemaphoreType.DMA((8,)),
         ],
         cost_estimate=pl.CostEstimate(
-            flops=4 * slot_rows * width * ff * tp_count,
-            bytes_accessed=12_000_000,
-            transcendentals=0,
+            flops=12 * slot_rows * width * ff, bytes_accessed=9_000_000, transcendentals=0
         ),
-        name="hidden_rows",
+        compiler_params=pltpu.CompilerParams(vmem_limit_bytes=24 * 2**20),
+        name="near_rows",
     )(
-        received, moe_gain.reshape(1, width),
-        gate, up, gate_r, up_r, gate_l, up_l, gate_f, up_f,
-    )
+        on_chip(received), moe_gain.reshape(1, width),
+        gate, up, *[on_chip(w) for w in (gate_r, up_r, gate_l, up_l)],
+    )
+    far_hidden, near_sum = pl.pallas_call(
+        far_kernel,
+        out_shape=[
+            kept_on_chip((slot_rows, ff)),
+            jax.ShapeDtypeStruct((slot_rows, width), jnp.float32),
+        ],
+        in_specs=[VMEM] * 7,
+        out_specs=[VMEM] * 2,
+        cost_estimate=pl.CostEstimate(
+            flops=10 * slot_rows * width * ff, bytes_accessed=9_000_000, transcendentals=0
+        ),
+        compiler_params=pltpu.CompilerParams(vmem_limit_bytes=16 * 2**20),
+        name="far_rows",
+    )(*[on_chip(v) for v in (normed, gate_f, up_f, near, down, down_r, down_l)])
     results = pl.pallas_call(
         down_kernel,
         out_shape=exchange_shape,
-        in_specs=[VMEM] + [ANY] * 5,
-        out_specs=VMEM,
+        in_specs=[VMEM] * 4,
+        out_specs=HBM,
         scratch_shapes=[
-            pltpu.VMEM((groups, tp_count * ff, LANES), jnp.bfloat16),
+            pltpu.VMEM((ep_count, 9 * groups, LANES), jnp.bfloat16),
             pltpu.VMEM((LANES // 128, ep_count * groups, 128), jnp.float32),
-            pltpu.SemaphoreType.DMA((5 * groups,)),
+            pltpu.SemaphoreType.DMA((groups + 1,)),
         ],
         cost_estimate=pl.CostEstimate(
-            flops=2 * slot_rows * width * ff * tp_count,
+            flops=2 * slot_rows * width * ff,
             bytes_accessed=8_000_000,
             transcendentals=0,
         ),
+        compiler_params=pltpu.CompilerParams(vmem_limit_bytes=56 * 2**20),
         name="down_rows",
-    )(hidden, down, down_r, down_l, down_fa, down_fb)
+    )(
+        *[
+            on_chip(v)
+            for v in (near_sum, far_hidden, down_fa, down_fb)
+        ]
+    )
     returned = lax.all_to_all(results, "ep", 0, 0, tiled=True)
     rows, head_width = queries.shape
     heads = head_width // HEAD
@@ -374,7 +442,7 @@
     own, right, left, far = pl.pallas_call(
         attention_kernel,
         out_shape=[quarter_shape] * 4,
-        in_specs=[SMEM, VMEM, VMEM, VMEM, VMEM, ANY],
+        in_specs=[SMEM] + [VMEM] * 11,
         out_specs=[VMEM] * 4,
         scratch_shapes=[
             pltpu.VMEM((heads, rows, 2 * HEAD), jnp.bfloat16),
@@ -385,8 +453,9 @@
         cost_estimate=pl.CostEstimate(
             flops=30_000_000_000, bytes_accessed=5_000_000, transcendentals=0
         ),
+        compiler_params=pltpu.CompilerParams(vmem_limit_bytes=28 * 2**20),
         name="attend_rows",
-    )(place, queries, all_pairs, log_gate_cum, mix_weight, results)
+    )(place, queries, log_gate_cum, mix_weight, *[on_chip(k) for k in core_keys + other_keys])
     from_left = lax.ppermute(right, "tp", to_right)
     from_right = lax.ppermute(left, "tp", to_left)
     from_far = lax.ppermute(far, "tp", to_far)
@@ -403,8 +472,9 @@
         in_specs=[VMEM, VMEM, VMEM],
         out_specs=VMEM,
         scratch_shapes=[pltpu.VMEM((LANES // 128, ep_count * groups, 128), jnp.float32)],
+        compiler_params=pltpu.CompilerParams(vmem_limit_bytes=16 * 2**20),
         name="combine_rows",
-    )(lane_routes, lane_weight, returned)
+    )(lane_routes, lane_weight, on_chip(returned))
     return (mix_result, moe_result)
 
 

time: 221 us -> 251 us (1.14); the launches traced: 220 us -> 247 us
  waiting for transfers between devices: 124 us -> 145 us
  starting transfers between devices: 39.5 us -> 60.3 us
  between operations: 14.2 us -> 0.87 us
  local copies, waits for them, and re-layouts: 3.98 us -> 16.9 us
  Pallas kernels: 34.8 us -> 23.1 us
    ppermute x0 -> x14, waiting for transfers between devices: none -> 65.4 us  [the longest x7 62 us: body(): lax.ppermute(keys_values, 'ep', shift_pairs(d, 0, 0))]
    ppermute x0 -> x14, starting transfers between devices: none -> 22.3 us  [the longest x7 12.6 us: body(): lax.ppermute(keys_values, 'ep', shift_pairs(d, 0, 0))]
    ppermute x1, waiting for transfers between devices: 20.8 us -> 0.01 us  [body(): gate_f = lax.ppermute(gate_r, 'tp', to_right)]
    ppermute x1, waiting for transfers between devices: 20.6 us -> 0.01 us  [body(): gate_r = lax.ppermute(gate, 'tp', to_right)]
    ppermute x1, waiting for transfers between devices: 19.6 us -> 0.01 us  [body(): down_r = lax.ppermute(down, 'tp', to_right)]
    ppermute x1, waiting for transfers between devices: 19.6 us -> 1.3 us  [body(): up_r = lax.ppermute(up, 'tp', to_right)]
    ppermute x1, waiting for transfers between devices: 0.01 us -> 15.3 us  [body(): down_l = lax.ppermute(down, 'tp', to_left)]
    ppermute x1, waiting for transfers between devices: 0.01 us -> 14.7 us  [body(): gate_l = lax.ppermute(gate, 'tp', to_left)]
  transfers between devices with their start and end apart: 16 -> 29, of which waited for: 9 -> 18; matrix products, arithmetic and copies ran while one was open for 2% -> 1% of each run, Pallas kernels for 14% -> 7%
where the time goes in v2:
time: 251 us; the launch traced here: 247 us
  waiting for transfers between devices  145 us (58%)
  starting transfers between devices  60.3 us (24%)
  Pallas kernels  23.1 us (9%)
  local copies, waits for them, and re-layouts  16.9 us (7%)
    ppermute x7, waiting for transfers between devices, body(): lax.ppermute(keys_values, 'ep', shift_pairs(d, 0, 0))  62 us
    all_to_all x1, waiting for transfers between devices, body(): returned = lax.all_to_all(results, 'ep', 0, 0, tiled=True)  24.4 us
    ppermute x1, waiting for transfers between devices, body(): down_l = lax.ppermute(down, 'tp', to_left)  15.3 us
    unnamed x60, local copies, waits for them, and re-layouts  15.2 us
    ppermute x1, waiting for transfers between devices, body(): gate_l = lax.ppermute(gate, 'tp', to_left)  14.7 us
    ppermute x7, starting transfers between devices, body(): lax.ppermute(keys_values, 'ep', shift_pairs(d, 0, 0))  12.6 us
    all_to_all x1, starting transfers between devices, body(): received = lax.all_to_all(outgoing, 'ep', 0, 0, tiled=True)  12.1 us
    ppermute x1, waiting for transfers between devices, body(): up_f = lax.ppermute(up_l, 'tp', to_left)  11.9 us
  transfers between devices with their start and end apart: 29, of which 18 were waited for; matrix products, arithmetic and copies ran while one was open for 1% of the time, Pallas kernels for 7%

profile of v2, /device:TPU:8, one launch (start us, length us, event | category | flops | bytes accessed | tf_op | source)
XLA Modules:
  0.0 247.3 jit_solution(6585565811379700341)
XLA Ops:
  2.4 2.4 dispatch_rows.1
  4.9 12.1 %all-to-all-start = ((bf16[64,72,256]{2,1,0:T(8,128)(2,1)}), bf16[64,72,256]{2,1,0:T(8,128)(2,1)S(1)}, u32[]{:S(2)}, u32[]{:S(2)}) async-start(bf16[64,72,256]{2,1,0:T(8,128)(2,1)} %dispatch_rows.1), calls=%async_computation | async-start | bytes 4718592 | tf_op jit(solution)/shard_map/all_to_all | solution.py:379
  22.2 2.4 collective-permute-start.1
  24.6 48.7 %collective-permute-done.refs_1_ = bf16[256,128]{1,0:T(8,128)(2,1)S(1)} collective-permute-done((bf16[256,128]{1,0:T(8,128)(2,1)S(1)}, bf16[256,128]{1,0:T(8,128)(2,1)S(1)}, u32[]{:S(2)}, u32[]{:S(2)}) %collective-permute-start) | collective-permute-done | bytes 65568 | tf_op jit(solution)/shard_map/ppermute | solution.py:350
  74.4 2.4 collective-permute-done.1.refs_2_
  78.3 3.0 %collective-permute-done.2.refs_3_ = bf16[256,128]{1,0:T(8,128)(2,1)S(1)} collective-permute-done((bf16[256,128]{1,0:T(8,128)(2,1)S(1)}, bf16[256,128]{1,0:T(8,128)(2,1)S(1)}, u32[]{:S(2)}, u32[]{:S(2)}) %collective-permute-start.2) | collective-permute-done | bytes 65568 | tf_op jit(solution)/shard_map/ppermute | solution.py:350
  81.3 4.2 %collective-permute-start.4 = (bf16[256,128]{1,0:T(8,128)(2,1)S(1)}, bf16[256,128]{1,0:T(8,128)(2,1)S(1)}, u32[]{:S(2)}, u32[]{:S(2)}) collective-permute-start(bf16[256,128]{1,0:T(8,128)(2,1)S(1)} %copy-done.5), channel_id=1, source_target_pairs={{0,160},{4,164},{8,168},{12,172},{16,176},{20,180},{24,184},{28,18... | collective-permute-start | bytes 196616 | tf_op jit(solution)/shard_map/ppermute | solution.py:350
  87.5 3.9 %collective-permute-done.4.refs_5_ = bf16[256,128]{1,0:T(8,128)(2,1)S(1)} collective-permute-done((bf16[256,128]{1,0:T(8,128)(2,1)S(1)}, bf16[256,128]{1,0:T(8,128)(2,1)S(1)}, u32[]{:S(2)}, u32[]{:S(2)}) %collective-permute-start.4) | collective-permute-done | bytes 65568 | tf_op jit(solution)/shard_map/ppermute | solution.py:350
  91.9 3.7 %collective-permute-done.6.refs_7_ = bf16[256,128]{1,0:T(8,128)(2,1)S(1)} collective-permute-done((bf16[256,128]{1,0:T(8,128)(2,1)S(1)}, bf16[256,128]{1,0:T(8,128)(2,1)S(1)}, u32[]{:S(2)}, u32[]{:S(2)}) %collective-permute-start.6) | collective-permute-done | bytes 65568 | tf_op jit(solution)/shard_map/ppermute | solution.py:350
  102.4 15.3 %collective-permute-done.24.d2 = bf16[256,2048]{1,0:T(8,128)(2,1)S(1)} collective-permute-done((bf16[256,2048]{1,0:T(8,128)(2,1)}, bf16[256,2048]{1,0:T(8,128)(2,1)S(1)}, u32[]{:S(2)}, u32[]{:S(2)}) %collective-permute-start.24) | collective-permute-done | bytes 1048608 | tf_op jit(solution)/shard_map/ppermute | solution.py:343
  117.7 2.0 collective-permute-start.7
  122.9 2.5 %collective-permute-start.8 = (bf16[2048,128]{1,0:T(8,128)(2,1)}, bf16[2048,128]{1,0:T(8,128)(2,1)}, u32[]{:S(2)}, u32[]{:S(2)}) collective-permute-start(bf16[2048,128]{1,0:T(8,128)(2,1)} %stack_rows.1.k0), channel_id=1, source_target_pairs={{0,24},{4,28},{8,0},{12,4},{16,8},{20,12},{24,16},{28,20},{32,56},... | collective-permute-start | bytes 1572872 | tf_op jit(solution)/shard_map/ppermute | solution.py:363
  125.5 14.7 %collective-permute-done.19.g2 = bf16[2048,256]{1,0:T(8,128)(2,1)S(1)} collective-permute-done((bf16[2048,256]{1,0:T(8,128)(2,1)S(1)}, bf16[2048,256]{1,0:T(8,128)(2,1)S(1)}, u32[]{:S(2)}, u32[]{:S(2)}) %collective-permute-start.19) | collective-permute-done | bytes 1048608 | tf_op jit(solution)/shard_map/ppermute | solution.py:341
  141.2 3.8 %collective-permute-start.9 = (bf16[2048,128]{1,0:T(8,128)(2,1)}, bf16[2048,128]{1,0:T(8,128)(2,1)}, u32[]{:S(2)}, u32[]{:S(2)}) collective-permute-start(bf16[2048,128]{1,0:T(8,128)(2,1)} %stack_rows.1.k0), channel_id=1, source_target_pairs={{0,16},{4,20},{8,24},{12,28},{16,0},{20,4},{24,8},{28,12},{32,48},... | collective-permute-start | bytes 1572872 | tf_op jit(solution)/shard_map/ppermute | solution.py:363
  147.7 11.9 %collective-permute-done.22.up = bf16[2048,256]{1,0:T(8,128)(2,1)S(1)} collective-permute-done((bf16[2048,256]{1,0:T(8,128)(2,1)S(1)}, bf16[2048,256]{1,0:T(8,128)(2,1)S(1)}, u32[]{:S(2)}, u32[]{:S(2)}) %collective-permute-start.22) | collective-permute-done | bytes 1048608 | tf_op jit(solution)/shard_map/ppermute | solution.py:345
  168.9 4.3 %near_rows.1 = (bf16[576,768]{1,0:T(8,128)(2,1)S(1)}, bf16[576,2048]{1,0:T(8,128)(2,1)S(1)}) custom-call(bf16[64,72,256]{2,1,0:T(8,128)(2,1)S(1)} %all-to-all-done.received_ref, f32[1,2048]{1,0:T(1,128)S(1)} %bitcast.22, bf16[2048,256]{1,0:T(8,128)(2,1)S(1)} %bitcast.15, bf16[2048,256]{1,0:T(8,128)(2,1)S(1)} %bitcast.18, bf16[2048,256]{1,0:T(8,128)(2,1)S(1)} %copy-done.15, ...), custom_call_target="tpu_custom_call" | custom-call | flops 3623878656 | bytes 9000000 | tf_op jit(solution)/shard_map/near_rows/pallas_call | solution.py:380
  173.3 3.2 %far_rows.1 = (bf16[576,256]{1,0:T(8,128)(2,1)S(1)}, f32[576,2048]{1,0:T(8,128)S(1)}) custom-call(bf16[576,2048]{1,0:T(8,128)(2,1)S(1)} %get-tuple-element.14.tokens_ref, bf16[2048,256]{1,0:T(8,128)(2,1)S(1)} %copy-done.23, bf16[2048,256]{1,0:T(8,128)(2,1)S(1)} %copy-done.25, bf16[576,768]{1,0:T(8,128)(2,1)S(1)} %get-tuple-element.15.near_ref, ...), custom_call_target="tpu_custom_call" | custom-call | flops 3019898880 | bytes 9000000 | tf_op jit(solution)/shard_map/far_rows/pallas_call | solution.py:400
  178.5 9.4 %all-to-all-start.1 = ((bf16[64,72,256]{2,1,0:T(8,128)(2,1)}), bf16[64,72,256]{2,1,0:T(8,128)(2,1)S(1)}, u32[]{:S(2)}, u32[]{:S(2)}) async-start(bf16[64,72,256]{2,1,0:T(8,128)(2,1)} %down_rows.1), calls=%async_computation.1 | async-start | bytes 4718592 | tf_op jit(solution)/shard_map/all_to_all | solution.py:437
  193.6 7.8 %attend_rows.1 = (bf16[64,2048]{1,0:T(8,128)(2,1)S(1)}, bf16[64,2048]{1,0:T(8,128)(2,1)S(1)}, bf16[64,2048]{1,0:T(8,128)(2,1)S(1)}, bf16[64,2048]{1,0:T(8,128)(2,1)S(1)}) custom-call(s32[4]{0:T(128)S(1)} %pad_add_fusion.place_ref, bf16[256,256]{1,0:T(8,128)(2,1)S(1)} %copy-done.27, f32[4,16384]{1,0:T(4,128)S(1)} %copy-done.26, ...), custom_call_target="tpu_custom_call" | custom-call | flops 30000001024 | bytes 5000000 | tf_op jit(solution)/shard_map/attend_rows/pallas_call | solution.py:442
  202.9 2.5 %collective-permute-start.15 = (bf16[64,2048]{1,0:T(8,128)(2,1)S(1)}, bf16[64,2048]{1,0:T(8,128)(2,1)S(1)}, u32[]{:S(2)}, u32[]{:S(2)}) collective-permute-start(bf16[64,2048]{1,0:T(8,128)(2,1)S(1)} %get-tuple-element.12), channel_id=1, source_target_pairs={{0,3},{1,0},{2,1},{3,2},{4,7},{5,4},{6,5},{7,6},{8,11},{9,8},{10,9... | collective-permute-start | bytes 786440 | tf_op jit(solution)/shard_map/ppermute | solution.py:460
  207.3 5.1 %collective-permute-done.14 = bf16[64,2048]{1,0:T(8,128)(2,1)S(1)} collective-permute-done((bf16[64,2048]{1,0:T(8,128)(2,1)S(1)}, bf16[64,2048]{1,0:T(8,128)(2,1)S(1)}, u32[]{:S(2)}, u32[]{:S(2)}) %collective-permute-start.14) | collective-permute-done | bytes 262176 | tf_op jit(solution)/shard_map/ppermute | solution.py:459
  212.4 6.9 %collective-permute-done.16 = bf16[64,2048]{1,0:T(8,128)(2,1)S(1)} collective-permute-done((bf16[64,2048]{1,0:T(8,128)(2,1)S(1)}, bf16[64,2048]{1,0:T(8,128)(2,1)S(1)}, u32[]{:S(2)}, u32[]{:S(2)}) %collective-permute-start.16) | collective-permute-done | bytes 262176 | tf_op jit(solution)/shard_map/ppermute | solution.py:461
  220.4 24.4 %all-to-all-done.1.returned_ref = bf16[64,72,256]{2,1,0:T(8,128)(2,1)S(1)} async-done(((bf16[64,72,256]{2,1,0:T(8,128)(2,1)}), bf16[64,72,256]{2,1,0:T(8,128)(2,1)S(1)}, u32[]{:S(2)}, u32[]{:S(2)}) %all-to-all-start.1) | async-done | bytes 2359328 | tf_op jit(solution)/shard_map/all_to_all | solution.py:437
  244.8 2.5 %combine_rows.1 = bf16[192,2048]{1,0:T(8,128)(2,1)} custom-call(s32[2,192]{1,0:T(2,128)S(1)} %bitcast.11, f32[2,192]{1,0:T(2,128)S(1)} %bitcast.12, bf16[64,72,256]{2,1,0:T(8,128)(2,1)S(1)} %all-to-all-done.1.returned_ref), custom_call_target="tpu_custom_call" | custom-call | tf_op jit(solution)/shard_map/combine_rows/pallas_call | solution.py:469
  (107 shorter events, 47.3 us)
Async XLA Ops:
  4.9 156.6 %all-to-all-start = ((bf16[64,72,256]{2,1,0:T(8,128)(2,1)}), bf16[64,72,256]{2,1,0:T(8,128)(2,1)S(1)}, u32[]{:S(2)}, u32[]{:S(2)}) async-start(bf16[64,72,256]{2,1,0:T(8,128)(2,1)} %dispatch_rows.1), calls=%async_computation | async-start | bytes 4718592 | tf_op jit(solution)/shard_map/all_to_all | solution.py:379
  17.0 80.3 %collective-permute-start.17 = (bf16[2048,256]{1,0:T(8,128)(2,1)S(1)}, bf16[2048,256]{1,0:T(8,128)(2,1)S(1)}, u32[]{:S(2)}, u32[]{:S(2)}) collective-permute-start(bf16[2048,256]{1,0:T(8,128)(2,1)S(1)} %bitcast.13), channel_id=1, source_target_pairs={{0,1},{1,2},{2,3},{3,0},{4,5},{5,6},{6,7},{7,4},{8,9},{9,10},{10,1... | collective-permute-start | bytes 3145736 | tf_op jit(solution)/shard_map/ppermute | solution.py:338
  18.6 79.1 %collective-permute-start.20 = (bf16[2048,256]{1,0:T(8,128)(2,1)}, bf16[2048,256]{1,0:T(8,128)(2,1)S(1)}, u32[]{:S(2)}, u32[]{:S(2)}) collective-permute-start(bf16[2048,256]{1,0:T(8,128)(2,1)} %bitcast.16), channel_id=1, source_target_pairs={{0,3},{1,0},{2,1},{3,2},{4,7},{5,4},{6,5},{7,6},{8,11},{9,8},{10,9... | collective-permute-start | bytes 3145736 | tf_op jit(solution)/shard_map/ppermute | solution.py:339
  19.1 80.2 %collective-permute-start.23 = (bf16[256,2048]{1,0:T(8,128)(2,1)}, bf16[256,2048]{1,0:T(8,128)(2,1)S(1)}, u32[]{:S(2)}, u32[]{:S(2)}) collective-permute-start(bf16[256,2048]{1,0:T(8,128)(2,1)} %bitcast.19), channel_id=1, source_target_pairs={{0,1},{1,2},{2,3},{3,0},{4,5},{5,6},{6,7},{7,4},{8,9},{9,10},{10,1... | collective-permute-start | bytes 3145736 | tf_op jit(solution)/shard_map/ppermute | solution.py:342
  20.7 52.7 %collective-permute-start = (bf16[256,128]{1,0:T(8,128)(2,1)S(1)}, bf16[256,128]{1,0:T(8,128)(2,1)S(1)}, u32[]{:S(2)}, u32[]{:S(2)}) collective-permute-start(bf16[256,128]{1,0:T(8,128)(2,1)S(1)} %copy-done.5), channel_id=1, source_target_pairs={{0,32},{4,36},{8,40},{12,44},{16,48},{20,52},{24,56},{28,60},{32,6... | collective-permute-start | bytes 196616 | tf_op jit(solution)/shard_map/ppermute | solution.py:350
  22.2 54.6 %collective-permute-start.1 = (bf16[256,128]{1,0:T(8,128)(2,1)S(1)}, bf16[256,128]{1,0:T(8,128)(2,1)S(1)}, u32[]{:S(2)}, u32[]{:S(2)}) collective-permute-start(bf16[256,128]{1,0:T(8,128)(2,1)S(1)} %copy-done.5), channel_id=1, source_target_pairs={{0,64},{4,68},{8,72},{12,76},{16,80},{20,84},{24,88},{28,92},{32,9... | collective-permute-start | bytes 196616 | tf_op jit(solution)/shard_map/ppermute | solution.py:350
  73.4 7.9 %collective-permute-start.2 = (bf16[256,128]{1,0:T(8,128)(2,1)S(1)}, bf16[256,128]{1,0:T(8,128)(2,1)S(1)}, u32[]{:S(2)}, u32[]{:S(2)}) collective-permute-start(bf16[256,128]{1,0:T(8,128)(2,1)S(1)} %copy-done.5), channel_id=1, source_target_pairs={{0,96},{4,100},{8,104},{12,108},{16,112},{20,116},{24,120},{28,124... | collective-permute-start | bytes 196616 | tf_op jit(solution)/shard_map/ppermute | solution.py:350
  76.8 8.8 %collective-permute-start.3 = (bf16[256,128]{1,0:T(8,128)(2,1)S(1)}, bf16[256,128]{1,0:T(8,128)(2,1)S(1)}, u32[]{:S(2)}, u32[]{:S(2)}) collective-permute-start(bf16[256,128]{1,0:T(8,128)(2,1)S(1)} %copy-done.5), channel_id=1, source_target_pairs={{0,128},{4,132},{8,136},{12,140},{16,144},{20,148},{24,152},{28,15... | collective-permute-start | bytes 196616 | tf_op jit(solution)/shard_map/ppermute | solution.py:350
  81.3 10.1 %collective-permute-start.4 = (bf16[256,128]{1,0:T(8,128)(2,1)S(1)}, bf16[256,128]{1,0:T(8,128)(2,1)S(1)}, u32[]{:S(2)}, u32[]{:S(2)}) collective-permute-start(bf16[256,128]{1,0:T(8,128)(2,1)S(1)} %copy-done.5), channel_id=1, source_target_pairs={{0,160},{4,164},{8,168},{12,172},{16,176},{20,180},{24,184},{28,18... | collective-permute-start | bytes 196616 | tf_op jit(solution)/shard_map/ppermute | solution.py:350
  85.6 5.9 %collective-permute-start.5 = (bf16[256,128]{1,0:T(8,128)(2,1)S(1)}, bf16[256,128]{1,0:T(8,128)(2,1)S(1)}, u32[]{:S(2)}, u32[]{:S(2)}) collective-permute-start(bf16[256,128]{1,0:T(8,128)(2,1)S(1)} %copy-done.5), channel_id=1, source_target_pairs={{0,192},{4,196},{8,200},{12,204},{16,208},{20,212},{24,216},{28,22... | collective-permute-start | bytes 196616 | tf_op jit(solution)/shard_map/ppermute | solution.py:350
  91.5 26.2 %collective-permute-start.24 = (bf16[256,2048]{1,0:T(8,128)(2,1)}, bf16[256,2048]{1,0:T(8,128)(2,1)S(1)}, u32[]{:S(2)}, u32[]{:S(2)}) collective-permute-start(bf16[256,2048]{1,0:T(8,128)(2,1)} %bitcast.20), channel_id=1, source_target_pairs={{0,3},{1,0},{2,1},{3,2},{4,7},{5,4},{6,5},{7,6},{8,11},{9,8},{10,9... | collective-permute-start | bytes 3145736 | tf_op jit(solution)/shard_map/ppermute | solution.py:343
  95.7 26.2 %collective-permute-start.18 = (bf16[2048,256]{1,0:T(8,128)(2,1)}, bf16[2048,256]{1,0:T(8,128)(2,1)S(1)}, u32[]{:S(2)}, u32[]{:S(2)}) collective-permute-start(bf16[2048,256]{1,0:T(8,128)(2,1)} %bitcast.17), channel_id=1, source_target_pairs={{0,1},{1,2},{2,3},{3,0},{4,5},{5,6},{6,7},{7,4},{8,9},{9,10},{10,1... | collective-permute-start | bytes 3145736 | tf_op jit(solution)/shard_map/ppermute | solution.py:340
  97.3 42.9 %collective-permute-start.19 = (bf16[2048,256]{1,0:T(8,128)(2,1)S(1)}, bf16[2048,256]{1,0:T(8,128)(2,1)S(1)}, u32[]{:S(2)}, u32[]{:S(2)}) collective-permute-start(bf16[2048,256]{1,0:T(8,128)(2,1)S(1)} %bitcast.14), channel_id=1, source_target_pairs={{0,3},{1,0},{2,1},{3,2},{4,7},{5,4},{6,5},{7,6},{8,11},{9,8},{10,9... | collective-permute-start | bytes 3145736 | tf_op jit(solution)/shard_map/ppermute | solution.py:341
  97.7 47.3 %collective-permute-start.21 = (bf16[2048,256]{1,0:T(8,128)(2,1)S(1)}, bf16[2048,256]{1,0:T(8,128)(2,1)S(1)}, u32[]{:S(2)}, u32[]{:S(2)}) collective-permute-start(bf16[2048,256]{1,0:T(8,128)(2,1)S(1)} %collective-permute-done.17.g1), channel_id=1, source_target_pairs={{0,1},{1,2},{2,3},{3,0},{4,5},{5,6},{6,7},{7,4},{8,9},{9,10},{10,1... | collective-permute-start | bytes 3145736 | tf_op jit(solution)/shard_map/ppermute | solution.py:344
  99.3 60.3 %collective-permute-start.22 = (bf16[2048,256]{1,0:T(8,128)(2,1)S(1)}, bf16[2048,256]{1,0:T(8,128)(2,1)S(1)}, u32[]{:S(2)}, u32[]{:S(2)}) collective-permute-start(bf16[2048,256]{1,0:T(8,128)(2,1)S(1)} %collective-permute-done.20.u2), channel_id=1, source_target_pairs={{0,3},{1,0},{2,1},{3,2},{4,7},{5,4},{6,5},{7,6},{8,11},{9,8},{10,9... | collective-permute-start | bytes 3145736 | tf_op jit(solution)/shard_map/ppermute | solution.py:345
  117.7 70.5 %collective-permute-start.7 = (bf16[2048,128]{1,0:T(8,128)(2,1)}, bf16[2048,128]{1,0:T(8,128)(2,1)}, u32[]{:S(2)}, u32[]{:S(2)}) collective-permute-start(bf16[2048,128]{1,0:T(8,128)(2,1)} %stack_rows.1.k0), channel_id=1, source_target_pairs={{0,8},{4,12},{8,16},{12,20},{16,24},{20,28},{24,0},{28,4},{32,40},... | collective-permute-start | bytes 1572872 | tf_op jit(solution)/shard_map/ppermute | solution.py:363
  122.9 65.7 %collective-permute-start.8 = (bf16[2048,128]{1,0:T(8,128)(2,1)}, bf16[2048,128]{1,0:T(8,128)(2,1)}, u32[]{:S(2)}, u32[]{:S(2)}) collective-permute-start(bf16[2048,128]{1,0:T(8,128)(2,1)} %stack_rows.1.k0), channel_id=1, source_target_pairs={{0,24},{4,28},{8,0},{12,4},{16,8},{20,12},{24,16},{28,20},{32,56},... | collective-permute-start | bytes 1572872 | tf_op jit(solution)/shard_map/ppermute | solution.py:363
  141.2 47.6 %collective-permute-start.9 = (bf16[2048,128]{1,0:T(8,128)(2,1)}, bf16[2048,128]{1,0:T(8,128)(2,1)}, u32[]{:S(2)}, u32[]{:S(2)}) collective-permute-start(bf16[2048,128]{1,0:T(8,128)(2,1)} %stack_rows.1.k0), channel_id=1, source_target_pairs={{0,16},{4,20},{8,24},{12,28},{16,0},{20,4},{24,8},{28,12},{32,48},... | collective-permute-start | bytes 1572872 | tf_op jit(solution)/shard_map/ppermute | solution.py:363
  146.1 30.4 %collective-permute-start.25 = (bf16[128,2048]{1,0:T(8,128)(2,1)}, bf16[128,2048]{1,0:T(8,128)(2,1)S(1)}, u32[]{:S(2)}, u32[]{:S(2)}) collective-permute-start(bf16[128,2048]{1,0:T(8,128)(2,1)} %slice.8), channel_id=1, source_target_pairs={{0,1},{1,2},{2,3},{3,0},{4,5},{5,6},{6,7},{7,4},{8,9},{9,10},{10,1... | collective-permute-start | bytes 1572872 | tf_op jit(solution)/shard_map/ppermute | solution.py:346
  160.5 16.0 %collective-permute-start.26 = (bf16[128,2048]{1,0:T(8,128)(2,1)}, bf16[128,2048]{1,0:T(8,128)(2,1)S(1)}, u32[]{:S(2)}, u32[]{:S(2)}) collective-permute-start(bf16[128,2048]{1,0:T(8,128)(2,1)} %slice.9), channel_id=1, source_target_pairs={{0,3},{1,0},{2,1},{3,2},{4,7},{5,4},{6,5},{7,6},{8,11},{9,8},{10,9... | collective-permute-start | bytes 1572872 | tf_op jit(solution)/shard_map/ppermute | solution.py:347
  178.5 66.3 %all-to-all-start.1 = ((bf16[64,72,256]{2,1,0:T(8,128)(2,1)}), bf16[64,72,256]{2,1,0:T(8,128)(2,1)S(1)}, u32[]{:S(2)}, u32[]{:S(2)}) async-start(bf16[64,72,256]{2,1,0:T(8,128)(2,1)} %down_rows.1), calls=%async_computation.1 | async-start | bytes 4718592 | tf_op jit(solution)/shard_map/all_to_all | solution.py:437
  201.5 10.9 %collective-permute-start.14 = (bf16[64,2048]{1,0:T(8,128)(2,1)S(1)}, bf16[64,2048]{1,0:T(8,128)(2,1)S(1)}, u32[]{:S(2)}, u32[]{:S(2)}) collective-permute-start(bf16[64,2048]{1,0:T(8,128)(2,1)S(1)} %get-tuple-element.11), channel_id=1, source_target_pairs={{0,1},{1,2},{2,3},{3,0},{4,5},{5,6},{6,7},{7,4},{8,9},{9,10},{10,1... | collective-permute-start | bytes 786440 | tf_op jit(solution)/shard_map/ppermute | solution.py:459
  202.9 9.5 %collective-permute-start.15 = (bf16[64,2048]{1,0:T(8,128)(2,1)S(1)}, bf16[64,2048]{1,0:T(8,128)(2,1)S(1)}, u32[]{:S(2)}, u32[]{:S(2)}) collective-permute-start(bf16[64,2048]{1,0:T(8,128)(2,1)S(1)} %get-tuple-element.12), channel_id=1, source_target_pairs={{0,3},{1,0},{2,1},{3,2},{4,7},{5,4},{6,5},{7,6},{8,11},{9,8},{10,9... | collective-permute-start | bytes 786440 | tf_op jit(solution)/shard_map/ppermute | solution.py:460
  205.3 13.9 %collective-permute-start.16 = (bf16[64,2048]{1,0:T(8,128)(2,1)S(1)}, bf16[64,2048]{1,0:T(8,128)(2,1)S(1)}, u32[]{:S(2)}, u32[]{:S(2)}) collective-permute-start(bf16[64,2048]{1,0:T(8,128)(2,1)S(1)} %get-tuple-element.13), channel_id=1, source_target_pairs={{0,2},{1,3},{2,0},{3,1},{4,6},{5,7},{6,4},{7,5},{8,10},{9,11},{10,... | collective-permute-start | bytes 786440 | tf_op jit(solution)/shard_map/ppermute | solution.py:461
  (35 other events, 531.7 us)

commit v3 on v2

--- a/solution.py
+++ b/solution.py
@@ -188,6 +188,8 @@
     sums_ref[...] = jnp.zeros_like(sums_ref)
     top_ref[...] = jnp.full_like(top_ref, NEGATIVE)
     own_index = plane * 8 + column * 2 + core
+    own_gates = gate_ref[:, pl.ds(pl.multiple_of(own_index * rows, rows), rows)]
+    base = own_gates[:, 0:1]
 
     def fold(pairs, gates, causal):
         lane = lax.broadcasted_iota(jnp.int32, pairs.shape, 1)
@@ -218,7 +220,7 @@
 
     fold(
         k0[:rows, :],
-        gate_ref[:, pl.ds(pl.multiple_of(own_index * rows, rows), rows)],
+        own_gates - base,
         lax.broadcasted_iota(jnp.int32, (rows, rows), 1)
         <= lax.broadcasted_iota(jnp.int32, (rows, rows), 0),
     )
@@ -231,7 +233,7 @@
                 index = (plane - back) * 8 + ((column + 4 - across) % 4) * 2 + (core + other) % 2
                 gate = gate_ref[:, pl.ds(pl.multiple_of(index * rows, rows), rows)]
                 pairs.append(keys[pl.ds(at, rows), :])
-                gates.append(jnp.where(index < own_index, gate, -NEGATIVE))
+                gates.append(jnp.where(index < own_index, gate - base, -NEGATIVE))
             fold(jnp.concatenate(pairs, axis=0), jnp.concatenate(gates, axis=1), None)
         return carry
 
@@ -249,22 +251,31 @@
         ).astype(jnp.bfloat16)
 
 
-def combine_kernel(routes_ref, weight_ref, returned_ref, out_ref, ninth_ref):
+def picks_kernel(routes_ref, weight_ref, eight_ref, ninth_ref, scale_ref):
+    experts = ninth_ref.shape[2]
+    tokens = routes_ref.shape[1]
+    row = lax.broadcasted_iota(jnp.int32, (tokens, tokens), 0)
+    col = lax.broadcasted_iota(jnp.int32, (tokens, tokens), 1)
+
+    def upright(lanes):
+        return jnp.sum(jnp.where(row == col, lanes, 0.0), axis=1, keepdims=True)
+
+    for k, (expert, place) in enumerate(slot_positions(routes_ref[...], experts)):
+        expert = upright(expert.astype(jnp.float32)).astype(jnp.int32)
+        place = upright(place.astype(jnp.float32)).astype(jnp.int32)
+        eight = lax.broadcasted_iota(jnp.int32, (tokens, experts * 8), 1)
+        ninth = lax.broadcasted_iota(jnp.int32, (tokens, experts), 1)
+        eight_ref[k] = as_bf16(eight == jnp.where(place < 8, expert * 8 + place, -1))
+        ninth_ref[k] = as_bf16(ninth == jnp.where(place == 8, expert, -1))
+        scale_ref[k] = jnp.broadcast_to(upright(weight_ref[k : k + 1, :]), scale_ref.shape[1:])
+
+
+def combine_kernel(eight_ref, last_ref, scale_ref, returned_ref, out_ref, ninth_ref):
     experts = returned_ref.shape[0]
     groups = returned_ref.shape[1] // 9
-    tokens = routes_ref.shape[1]
-    picks = slot_positions(routes_ref[...], experts)
-    masks = [[as_bf16(m) for m in slot_masks(e, p, experts)] for e, p in picks]
-    row = lax.broadcasted_iota(jnp.int32, (tokens, tokens), 0)
-    col = lax.broadcasted_iota(jnp.int32, (tokens, tokens), 1)
-    weights = [
-        jnp.sum(jnp.where(row == col, weight_ref[k : k + 1, :], 0.0), axis=1, keepdims=True)
-        for k in range(2)
-    ]
     ninth = returned_ref[:, 8 * groups :, :].astype(jnp.float32).reshape(experts * groups, LANES)
     for h in range(LANES // 128):
         ninth_ref[h] = ninth[:, h * 128 : (h + 1) * 128]
-    over_slots = (((0,), (0,)), ((), ()))
     for g in range(groups):
         eight = as_rows(returned_ref[:, g * 8 : (g + 1) * 8, :])
         last = jnp.concatenate(
@@ -272,10 +283,10 @@
         ).astype(jnp.bfloat16)
         total = 0.0
         for k in range(2):
-            chosen = lax.dot_general(
-                masks[k][0], eight, over_slots, preferred_element_type=jnp.float32
-            ) + lax.dot_general(masks[k][1], last, over_slots, preferred_element_type=jnp.float32)
-            total = total + weights[k] * chosen
+            chosen = jnp.dot(eight_ref[k], eight, preferred_element_type=jnp.float32) + jnp.dot(
+                last_ref[k], last, preferred_element_type=jnp.float32
+            )
+            total = total + scale_ref[k][:, 0:1] * chosen
         out_ref[:, g * LANES : (g + 1) * LANES] = total.astype(jnp.bfloat16)
 
 
@@ -466,15 +477,27 @@
         + from_far.astype(jnp.float32)
     )
     mix_result = rms_scale(projected, mix_gain).astype(jnp.bfloat16)
+    masks = pl.pallas_call(
+        picks_kernel,
+        out_shape=[
+            jax.ShapeDtypeStruct((2, rows_here, ep_count * 8), jnp.bfloat16),
+            jax.ShapeDtypeStruct((2, rows_here, ep_count), jnp.bfloat16),
+            jax.ShapeDtypeStruct((2, rows_here, 128), jnp.float32),
+        ],
+        in_specs=[VMEM] * 2,
+        out_specs=[VMEM] * 3,
+        compiler_params=pltpu.CompilerParams(vmem_limit_bytes=12 * 2**20),
+        name="pick_masks",
+    )(lane_routes, lane_weight)
     moe_result = pl.pallas_call(
         combine_kernel,
         out_shape=jax.ShapeDtypeStruct((rows_here, width), jnp.bfloat16),
-        in_specs=[VMEM, VMEM, VMEM],
+        in_specs=[VMEM] * 4,
         out_specs=VMEM,
         scratch_shapes=[pltpu.VMEM((LANES // 128, ep_count * groups, 128), jnp.float32)],
         compiler_params=pltpu.CompilerParams(vmem_limit_bytes=16 * 2**20),
         name="combine_rows",
-    )(lane_routes, lane_weight, on_chip(returned))
+    )(*[on_chip(m) for m in masks], on_chip(returned))
     return (mix_result, moe_result)
 
 

time: 251 us -> 251 us (level)
  transfers between devices with their start and end apart: 29 -> 29, of which waited for: 18 -> 18; matrix products, arithmetic and copies ran while one was open for 1% -> 1% of each run, Pallas kernels for 7% -> 8%
where the time goes in v3:
time: 251 us; the launch traced here: 247 us
  waiting for transfers between devices  145 us (58%)
  starting transfers between devices  60.3 us (24%)
  Pallas kernels  23.3 us (9%)
  local copies, waits for them, and re-layouts  16.9 us (7%)
    ppermute x7, waiting for transfers between devices, body(): lax.ppermute(keys_values, 'ep', shift_pairs(d, 0, 0))  62 us
    all_to_all x1, waiting for transfers between devices, body(): returned = lax.all_to_all(results, 'ep', 0, 0, tiled=True)  24.4 us
    ppermute x1, waiting for transfers between devices, body(): down_l = lax.ppermute(down, 'tp', to_left)  15.3 us
    unnamed x60, local copies, waits for them, and re-layouts  15.2 us
    ppermute x1, waiting for transfers between devices, body(): gate_l = lax.ppermute(gate, 'tp', to_left)  14.7 us
    ppermute x7, starting transfers between devices, body(): lax.ppermute(keys_values, 'ep', shift_pairs(d, 0, 0))  12.6 us
    all_to_all x1, starting transfers between devices, body(): received = lax.all_to_all(outgoing, 'ep', 0, 0, tiled=True)  12.1 us
    ppermute x1, waiting for transfers between devices, body(): up_f = lax.ppermute(up_l, 'tp', to_left)  11.9 us
  transfers between devices with their start and end apart: 29, of which 18 were waited for; matrix products, arithmetic and copies ran while one was open for 1% of the time, Pallas kernels for 8%

profile of v3, /device:TPU:8, one launch (start us, length us, event | category | flops | bytes accessed | tf_op | source)
XLA Modules:
  0.0 247.2 jit_solution(10164618554466866031)
XLA Ops:
  2.4 2.4 dispatch_rows.1
  4.9 12.1 %all-to-all-start = ((bf16[64,72,256]{2,1,0:T(8,128)(2,1)}), bf16[64,72,256]{2,1,0:T(8,128)(2,1)S(1)}, u32[]{:S(2)}, u32[]{:S(2)}) async-start(bf16[64,72,256]{2,1,0:T(8,128)(2,1)} %dispatch_rows.1), calls=%async_computation | async-start | bytes 4718592 | tf_op jit(solution)/shard_map/all_to_all | solution.py:390
  22.2 2.4 collective-permute-start.1
  24.6 48.7 %collective-permute-done.refs_1_ = bf16[256,128]{1,0:T(8,128)(2,1)S(1)} collective-permute-done((bf16[256,128]{1,0:T(8,128)(2,1)S(1)}, bf16[256,128]{1,0:T(8,128)(2,1)S(1)}, u32[]{:S(2)}, u32[]{:S(2)}) %collective-permute-start) | collective-permute-done | bytes 65568 | tf_op jit(solution)/shard_map/ppermute | solution.py:361
  74.4 2.4 collective-permute-done.1.refs_2_
  78.3 3.0 %collective-permute-done.2.refs_3_ = bf16[256,128]{1,0:T(8,128)(2,1)S(1)} collective-permute-done((bf16[256,128]{1,0:T(8,128)(2,1)S(1)}, bf16[256,128]{1,0:T(8,128)(2,1)S(1)}, u32[]{:S(2)}, u32[]{:S(2)}) %collective-permute-start.2) | collective-permute-done | bytes 65568 | tf_op jit(solution)/shard_map/ppermute | solution.py:361
  81.3 4.2 %collective-permute-start.4 = (bf16[256,128]{1,0:T(8,128)(2,1)S(1)}, bf16[256,128]{1,0:T(8,128)(2,1)S(1)}, u32[]{:S(2)}, u32[]{:S(2)}) collective-permute-start(bf16[256,128]{1,0:T(8,128)(2,1)S(1)} %copy-done.5), channel_id=1, source_target_pairs={{0,160},{4,164},{8,168},{12,172},{16,176},{20,180},{24,184},{28,18... | collective-permute-start | bytes 196616 | tf_op jit(solution)/shard_map/ppermute | solution.py:361
  87.5 3.9 %collective-permute-done.4.refs_5_ = bf16[256,128]{1,0:T(8,128)(2,1)S(1)} collective-permute-done((bf16[256,128]{1,0:T(8,128)(2,1)S(1)}, bf16[256,128]{1,0:T(8,128)(2,1)S(1)}, u32[]{:S(2)}, u32[]{:S(2)}) %collective-permute-start.4) | collective-permute-done | bytes 65568 | tf_op jit(solution)/shard_map/ppermute | solution.py:361
  91.9 3.7 %collective-permute-done.6.refs_7_ = bf16[256,128]{1,0:T(8,128)(2,1)S(1)} collective-permute-done((bf16[256,128]{1,0:T(8,128)(2,1)S(1)}, bf16[256,128]{1,0:T(8,128)(2,1)S(1)}, u32[]{:S(2)}, u32[]{:S(2)}) %collective-permute-start.6) | collective-permute-done | bytes 65568 | tf_op jit(solution)/shard_map/ppermute | solution.py:361
  102.4 15.3 %collective-permute-done.24.d2 = bf16[256,2048]{1,0:T(8,128)(2,1)S(1)} collective-permute-done((bf16[256,2048]{1,0:T(8,128)(2,1)}, bf16[256,2048]{1,0:T(8,128)(2,1)S(1)}, u32[]{:S(2)}, u32[]{:S(2)}) %collective-permute-start.24) | collective-permute-done | bytes 1048608 | tf_op jit(solution)/shard_map/ppermute | solution.py:354
  117.7 2.0 collective-permute-start.7
  122.9 2.5 %collective-permute-start.8 = (bf16[2048,128]{1,0:T(8,128)(2,1)}, bf16[2048,128]{1,0:T(8,128)(2,1)}, u32[]{:S(2)}, u32[]{:S(2)}) collective-permute-start(bf16[2048,128]{1,0:T(8,128)(2,1)} %stack_rows.1.k0), channel_id=1, source_target_pairs={{0,24},{4,28},{8,0},{12,4},{16,8},{20,12},{24,16},{28,20},{32,56},... | collective-permute-start | bytes 1572872 | tf_op jit(solution)/shard_map/ppermute | solution.py:374
  125.5 14.7 %collective-permute-done.19.g2 = bf16[2048,256]{1,0:T(8,128)(2,1)S(1)} collective-permute-done((bf16[2048,256]{1,0:T(8,128)(2,1)S(1)}, bf16[2048,256]{1,0:T(8,128)(2,1)S(1)}, u32[]{:S(2)}, u32[]{:S(2)}) %collective-permute-start.19) | collective-permute-done | bytes 1048608 | tf_op jit(solution)/shard_map/ppermute | solution.py:352
  141.2 3.8 %collective-permute-start.9 = (bf16[2048,128]{1,0:T(8,128)(2,1)}, bf16[2048,128]{1,0:T(8,128)(2,1)}, u32[]{:S(2)}, u32[]{:S(2)}) collective-permute-start(bf16[2048,128]{1,0:T(8,128)(2,1)} %stack_rows.1.k0), channel_id=1, source_target_pairs={{0,16},{4,20},{8,24},{12,28},{16,0},{20,4},{24,8},{28,12},{32,48},... | collective-permute-start | bytes 1572872 | tf_op jit(solution)/shard_map/ppermute | solution.py:374
  147.7 11.9 %collective-permute-done.22.up = bf16[2048,256]{1,0:T(8,128)(2,1)S(1)} collective-permute-done((bf16[2048,256]{1,0:T(8,128)(2,1)S(1)}, bf16[2048,256]{1,0:T(8,128)(2,1)S(1)}, u32[]{:S(2)}, u32[]{:S(2)}) %collective-permute-start.22) | collective-permute-done | bytes 1048608 | tf_op jit(solution)/shard_map/ppermute | solution.py:356
  168.9 4.3 %near_rows.1 = (bf16[576,768]{1,0:T(8,128)(2,1)S(1)}, bf16[576,2048]{1,0:T(8,128)(2,1)S(1)}) custom-call(bf16[64,72,256]{2,1,0:T(8,128)(2,1)S(1)} %all-to-all-done.received_ref, f32[1,2048]{1,0:T(1,128)S(1)} %bitcast.22, bf16[2048,256]{1,0:T(8,128)(2,1)S(1)} %bitcast.15, bf16[2048,256]{1,0:T(8,128)(2,1)S(1)} %bitcast.18, bf16[2048,256]{1,0:T(8,128)(2,1)S(1)} %copy-done.15, ...), custom_call_target="tpu_custom_call" | custom-call | flops 3623878656 | bytes 9000000 | tf_op jit(solution)/shard_map/near_rows/pallas_call | solution.py:391
  173.3 3.2 %far_rows.1 = (bf16[576,256]{1,0:T(8,128)(2,1)S(1)}, f32[576,2048]{1,0:T(8,128)S(1)}) custom-call(bf16[576,2048]{1,0:T(8,128)(2,1)S(1)} %get-tuple-element.20.tokens_ref, bf16[2048,256]{1,0:T(8,128)(2,1)S(1)} %copy-done.23, bf16[2048,256]{1,0:T(8,128)(2,1)S(1)} %copy-done.25, bf16[576,768]{1,0:T(8,128)(2,1)S(1)} %get-tuple-element.21.near_ref, ...), custom_call_target="tpu_custom_call" | custom-call | flops 3019898880 | bytes 9000000 | tf_op jit(solution)/shard_map/far_rows/pallas_call | solution.py:411
  178.5 9.4 %all-to-all-start.1 = ((bf16[64,72,256]{2,1,0:T(8,128)(2,1)}), bf16[64,72,256]{2,1,0:T(8,128)(2,1)S(1)}, u32[]{:S(2)}, u32[]{:S(2)}) async-start(bf16[64,72,256]{2,1,0:T(8,128)(2,1)} %down_rows.1), calls=%async_computation.1 | async-start | bytes 4718592 | tf_op jit(solution)/shard_map/all_to_all | solution.py:448
  193.7 7.8 %attend_rows.1 = (bf16[64,2048]{1,0:T(8,128)(2,1)S(1)}, bf16[64,2048]{1,0:T(8,128)(2,1)S(1)}, bf16[64,2048]{1,0:T(8,128)(2,1)S(1)}, bf16[64,2048]{1,0:T(8,128)(2,1)S(1)}) custom-call(s32[4]{0:T(128)S(1)} %pad_add_fusion.place_ref, bf16[256,256]{1,0:T(8,128)(2,1)S(1)} %copy-done.27, f32[4,16384]{1,0:T(4,128)S(1)} %copy-done.26, ...), custom_call_target="tpu_custom_call" | custom-call | flops 30000001024 | bytes 5000000 | tf_op jit(solution)/shard_map/attend_rows/pallas_call | solution.py:453
  202.9 2.5 %collective-permute-start.15 = (bf16[64,2048]{1,0:T(8,128)(2,1)S(1)}, bf16[64,2048]{1,0:T(8,128)(2,1)S(1)}, u32[]{:S(2)}, u32[]{:S(2)}) collective-permute-start(bf16[64,2048]{1,0:T(8,128)(2,1)S(1)} %get-tuple-element.15), channel_id=1, source_target_pairs={{0,3},{1,0},{2,1},{3,2},{4,7},{5,4},{6,5},{7,6},{8,11},{9,8},{10,9... | collective-permute-start | bytes 786440 | tf_op jit(solution)/shard_map/ppermute | solution.py:471
  207.7 4.7 %collective-permute-done.14 = bf16[64,2048]{1,0:T(8,128)(2,1)S(1)} collective-permute-done((bf16[64,2048]{1,0:T(8,128)(2,1)S(1)}, bf16[64,2048]{1,0:T(8,128)(2,1)S(1)}, u32[]{:S(2)}, u32[]{:S(2)}) %collective-permute-start.14) | collective-permute-done | bytes 262176 | tf_op jit(solution)/shard_map/ppermute | solution.py:470
  212.4 6.8 %collective-permute-done.16 = bf16[64,2048]{1,0:T(8,128)(2,1)S(1)} collective-permute-done((bf16[64,2048]{1,0:T(8,128)(2,1)S(1)}, bf16[64,2048]{1,0:T(8,128)(2,1)S(1)}, u32[]{:S(2)}, u32[]{:S(2)}) %collective-permute-start.16) | collective-permute-done | bytes 262176 | tf_op jit(solution)/shard_map/ppermute | solution.py:472
  220.4 24.4 %all-to-all-done.1.returned_ref = bf16[64,72,256]{2,1,0:T(8,128)(2,1)S(1)} async-done(((bf16[64,72,256]{2,1,0:T(8,128)(2,1)}), bf16[64,72,256]{2,1,0:T(8,128)(2,1)S(1)}, u32[]{:S(2)}, u32[]{:S(2)}) %all-to-all-start.1) | async-done | bytes 2359328 | tf_op jit(solution)/shard_map/all_to_all | solution.py:448
  244.9 2.3 combine_rows.1
  (108 shorter events, 47.7 us)
Async XLA Ops:
  4.9 156.6 %all-to-all-start = ((bf16[64,72,256]{2,1,0:T(8,128)(2,1)}), bf16[64,72,256]{2,1,0:T(8,128)(2,1)S(1)}, u32[]{:S(2)}, u32[]{:S(2)}) async-start(bf16[64,72,256]{2,1,0:T(8,128)(2,1)} %dispatch_rows.1), calls=%async_computation | async-start | bytes 4718592 | tf_op jit(solution)/shard_map/all_to_all | solution.py:390
  17.0 80.3 %collective-permute-start.17 = (bf16[2048,256]{1,0:T(8,128)(2,1)S(1)}, bf16[2048,256]{1,0:T(8,128)(2,1)S(1)}, u32[]{:S(2)}, u32[]{:S(2)}) collective-permute-start(bf16[2048,256]{1,0:T(8,128)(2,1)S(1)} %bitcast.13), channel_id=1, source_target_pairs={{0,1},{1,2},{2,3},{3,0},{4,5},{5,6},{6,7},{7,4},{8,9},{9,10},{10,1... | collective-permute-start | bytes 3145736 | tf_op jit(solution)/shard_map/ppermute | solution.py:349
  18.6 79.1 %collective-permute-start.20 = (bf16[2048,256]{1,0:T(8,128)(2,1)}, bf16[2048,256]{1,0:T(8,128)(2,1)S(1)}, u32[]{:S(2)}, u32[]{:S(2)}) collective-permute-start(bf16[2048,256]{1,0:T(8,128)(2,1)} %bitcast.16), channel_id=1, source_target_pairs={{0,3},{1,0},{2,1},{3,2},{4,7},{5,4},{6,5},{7,6},{8,11},{9,8},{10,9... | collective-permute-start | bytes 3145736 | tf_op jit(solution)/shard_map/ppermute | solution.py:350
  19.1 80.2 %collective-permute-start.23 = (bf16[256,2048]{1,0:T(8,128)(2,1)}, bf16[256,2048]{1,0:T(8,128)(2,1)S(1)}, u32[]{:S(2)}, u32[]{:S(2)}) collective-permute-start(bf16[256,2048]{1,0:T(8,128)(2,1)} %bitcast.19), channel_id=1, source_target_pairs={{0,1},{1,2},{2,3},{3,0},{4,5},{5,6},{6,7},{7,4},{8,9},{9,10},{10,1... | collective-permute-start | bytes 3145736 | tf_op jit(solution)/shard_map/ppermute | solution.py:353
  20.7 52.7 %collective-permute-start = (bf16[256,128]{1,0:T(8,128)(2,1)S(1)}, bf16[256,128]{1,0:T(8,128)(2,1)S(1)}, u32[]{:S(2)}, u32[]{:S(2)}) collective-permute-start(bf16[256,128]{1,0:T(8,128)(2,1)S(1)} %copy-done.5), channel_id=1, source_target_pairs={{0,32},{4,36},{8,40},{12,44},{16,48},{20,52},{24,56},{28,60},{32,6... | collective-permute-start | bytes 196616 | tf_op jit(solution)/shard_map/ppermute | solution.py:361
  22.2 54.6 %collective-permute-start.1 = (bf16[256,128]{1,0:T(8,128)(2,1)S(1)}, bf16[256,128]{1,0:T(8,128)(2,1)S(1)}, u32[]{:S(2)}, u32[]{:S(2)}) collective-permute-start(bf16[256,128]{1,0:T(8,128)(2,1)S(1)} %copy-done.5), channel_id=1, source_target_pairs={{0,64},{4,68},{8,72},{12,76},{16,80},{20,84},{24,88},{28,92},{32,9... | collective-permute-start | bytes 196616 | tf_op jit(solution)/shard_map/ppermute | solution.py:361
  73.4 7.9 %collective-permute-start.2 = (bf16[256,128]{1,0:T(8,128)(2,1)S(1)}, bf16[256,128]{1,0:T(8,128)(2,1)S(1)}, u32[]{:S(2)}, u32[]{:S(2)}) collective-permute-start(bf16[256,128]{1,0:T(8,128)(2,1)S(1)} %copy-done.5), channel_id=1, source_target_pairs={{0,96},{4,100},{8,104},{12,108},{16,112},{20,116},{24,120},{28,124... | collective-permute-start | bytes 196616 | tf_op jit(solution)/shard_map/ppermute | solution.py:361
  76.8 8.8 %collective-permute-start.3 = (bf16[256,128]{1,0:T(8,128)(2,1)S(1)}, bf16[256,128]{1,0:T(8,128)(2,1)S(1)}, u32[]{:S(2)}, u32[]{:S(2)}) collective-permute-start(bf16[256,128]{1,0:T(8,128)(2,1)S(1)} %copy-done.5), channel_id=1, source_target_pairs={{0,128},{4,132},{8,136},{12,140},{16,144},{20,148},{24,152},{28,15... | collective-permute-start | bytes 196616 | tf_op jit(solution)/shard_map/ppermute | solution.py:361
  81.3 10.1 %collective-permute-start.4 = (bf16[256,128]{1,0:T(8,128)(2,1)S(1)}, bf16[256,128]{1,0:T(8,128)(2,1)S(1)}, u32[]{:S(2)}, u32[]{:S(2)}) collective-permute-start(bf16[256,128]{1,0:T(8,128)(2,1)S(1)} %copy-done.5), channel_id=1, source_target_pairs={{0,160},{4,164},{8,168},{12,172},{16,176},{20,180},{24,184},{28,18... | collective-permute-start | bytes 196616 | tf_op jit(solution)/shard_map/ppermute | solution.py:361
  85.6 5.9 %collective-permute-start.5 = (bf16[256,128]{1,0:T(8,128)(2,1)S(1)}, bf16[256,128]{1,0:T(8,128)(2,1)S(1)}, u32[]{:S(2)}, u32[]{:S(2)}) collective-permute-start(bf16[256,128]{1,0:T(8,128)(2,1)S(1)} %copy-done.5), channel_id=1, source_target_pairs={{0,192},{4,196},{8,200},{12,204},{16,208},{20,212},{24,216},{28,22... | collective-permute-start | bytes 196616 | tf_op jit(solution)/shard_map/ppermute | solution.py:361
  91.5 26.2 %collective-permute-start.24 = (bf16[256,2048]{1,0:T(8,128)(2,1)}, bf16[256,2048]{1,0:T(8,128)(2,1)S(1)}, u32[]{:S(2)}, u32[]{:S(2)}) collective-permute-start(bf16[256,2048]{1,0:T(8,128)(2,1)} %bitcast.20), channel_id=1, source_target_pairs={{0,3},{1,0},{2,1},{3,2},{4,7},{5,4},{6,5},{7,6},{8,11},{9,8},{10,9... | collective-permute-start | bytes 3145736 | tf_op jit(solution)/shard_map/ppermute | solution.py:354
  95.7 26.2 %collective-permute-start.18 = (bf16[2048,256]{1,0:T(8,128)(2,1)}, bf16[2048,256]{1,0:T(8,128)(2,1)S(1)}, u32[]{:S(2)}, u32[]{:S(2)}) collective-permute-start(bf16[2048,256]{1,0:T(8,128)(2,1)} %bitcast.17), channel_id=1, source_target_pairs={{0,1},{1,2},{2,3},{3,0},{4,5},{5,6},{6,7},{7,4},{8,9},{9,10},{10,1... | collective-permute-start | bytes 3145736 | tf_op jit(solution)/shard_map/ppermute | solution.py:351
  97.3 42.9 %collective-permute-start.19 = (bf16[2048,256]{1,0:T(8,128)(2,1)S(1)}, bf16[2048,256]{1,0:T(8,128)(2,1)S(1)}, u32[]{:S(2)}, u32[]{:S(2)}) collective-permute-start(bf16[2048,256]{1,0:T(8,128)(2,1)S(1)} %bitcast.14), channel_id=1, source_target_pairs={{0,3},{1,0},{2,1},{3,2},{4,7},{5,4},{6,5},{7,6},{8,11},{9,8},{10,9... | collective-permute-start | bytes 3145736 | tf_op jit(solution)/shard_map/ppermute | solution.py:352
  97.7 47.3 %collective-permute-start.21 = (bf16[2048,256]{1,0:T(8,128)(2,1)S(1)}, bf16[2048,256]{1,0:T(8,128)(2,1)S(1)}, u32[]{:S(2)}, u32[]{:S(2)}) collective-permute-start(bf16[2048,256]{1,0:T(8,128)(2,1)S(1)} %collective-permute-done.17.g1), channel_id=1, source_target_pairs={{0,1},{1,2},{2,3},{3,0},{4,5},{5,6},{6,7},{7,4},{8,9},{9,10},{10,1... | collective-permute-start | bytes 3145736 | tf_op jit(solution)/shard_map/ppermute | solution.py:355
  99.3 60.3 %collective-permute-start.22 = (bf16[2048,256]{1,0:T(8,128)(2,1)S(1)}, bf16[2048,256]{1,0:T(8,128)(2,1)S(1)}, u32[]{:S(2)}, u32[]{:S(2)}) collective-permute-start(bf16[2048,256]{1,0:T(8,128)(2,1)S(1)} %collective-permute-done.20.u2), channel_id=1, source_target_pairs={{0,3},{1,0},{2,1},{3,2},{4,7},{5,4},{6,5},{7,6},{8,11},{9,8},{10,9... | collective-permute-start | bytes 3145736 | tf_op jit(solution)/shard_map/ppermute | solution.py:356
  117.7 70.5 %collective-permute-start.7 = (bf16[2048,128]{1,0:T(8,128)(2,1)}, bf16[2048,128]{1,0:T(8,128)(2,1)}, u32[]{:S(2)}, u32[]{:S(2)}) collective-permute-start(bf16[2048,128]{1,0:T(8,128)(2,1)} %stack_rows.1.k0), channel_id=1, source_target_pairs={{0,8},{4,12},{8,16},{12,20},{16,24},{20,28},{24,0},{28,4},{32,40},... | collective-permute-start | bytes 1572872 | tf_op jit(solution)/shard_map/ppermute | solution.py:374
  122.9 65.8 %collective-permute-start.8 = (bf16[2048,128]{1,0:T(8,128)(2,1)}, bf16[2048,128]{1,0:T(8,128)(2,1)}, u32[]{:S(2)}, u32[]{:S(2)}) collective-permute-start(bf16[2048,128]{1,0:T(8,128)(2,1)} %stack_rows.1.k0), channel_id=1, source_target_pairs={{0,24},{4,28},{8,0},{12,4},{16,8},{20,12},{24,16},{28,20},{32,56},... | collective-permute-start | bytes 1572872 | tf_op jit(solution)/shard_map/ppermute | solution.py:374
  141.2 47.6 %collective-permute-start.9 = (bf16[2048,128]{1,0:T(8,128)(2,1)}, bf16[2048,128]{1,0:T(8,128)(2,1)}, u32[]{:S(2)}, u32[]{:S(2)}) collective-permute-start(bf16[2048,128]{1,0:T(8,128)(2,1)} %stack_rows.1.k0), channel_id=1, source_target_pairs={{0,16},{4,20},{8,24},{12,28},{16,0},{20,4},{24,8},{28,12},{32,48},... | collective-permute-start | bytes 1572872 | tf_op jit(solution)/shard_map/ppermute | solution.py:374
  146.1 30.4 %collective-permute-start.25 = (bf16[128,2048]{1,0:T(8,128)(2,1)}, bf16[128,2048]{1,0:T(8,128)(2,1)S(1)}, u32[]{:S(2)}, u32[]{:S(2)}) collective-permute-start(bf16[128,2048]{1,0:T(8,128)(2,1)} %slice.8), channel_id=1, source_target_pairs={{0,1},{1,2},{2,3},{3,0},{4,5},{5,6},{6,7},{7,4},{8,9},{9,10},{10,1... | collective-permute-start | bytes 1572872 | tf_op jit(solution)/shard_map/ppermute | solution.py:357
  160.5 16.0 %collective-permute-start.26 = (bf16[128,2048]{1,0:T(8,128)(2,1)}, bf16[128,2048]{1,0:T(8,128)(2,1)S(1)}, u32[]{:S(2)}, u32[]{:S(2)}) collective-permute-start(bf16[128,2048]{1,0:T(8,128)(2,1)} %slice.9), channel_id=1, source_target_pairs={{0,3},{1,0},{2,1},{3,2},{4,7},{5,4},{6,5},{7,6},{8,11},{9,8},{10,9... | collective-permute-start | bytes 1572872 | tf_op jit(solution)/shard_map/ppermute | solution.py:358
  178.5 66.3 %all-to-all-start.1 = ((bf16[64,72,256]{2,1,0:T(8,128)(2,1)}), bf16[64,72,256]{2,1,0:T(8,128)(2,1)S(1)}, u32[]{:S(2)}, u32[]{:S(2)}) async-start(bf16[64,72,256]{2,1,0:T(8,128)(2,1)} %down_rows.1), calls=%async_computation.1 | async-start | bytes 4718592 | tf_op jit(solution)/shard_map/all_to_all | solution.py:448
  201.5 10.9 %collective-permute-start.14 = (bf16[64,2048]{1,0:T(8,128)(2,1)S(1)}, bf16[64,2048]{1,0:T(8,128)(2,1)S(1)}, u32[]{:S(2)}, u32[]{:S(2)}) collective-permute-start(bf16[64,2048]{1,0:T(8,128)(2,1)S(1)} %get-tuple-element.14), channel_id=1, source_target_pairs={{0,1},{1,2},{2,3},{3,0},{4,5},{5,6},{6,7},{7,4},{8,9},{9,10},{10,1... | collective-permute-start | bytes 786440 | tf_op jit(solution)/shard_map/ppermute | solution.py:470
  202.9 9.5 %collective-permute-start.15 = (bf16[64,2048]{1,0:T(8,128)(2,1)S(1)}, bf16[64,2048]{1,0:T(8,128)(2,1)S(1)}, u32[]{:S(2)}, u32[]{:S(2)}) collective-permute-start(bf16[64,2048]{1,0:T(8,128)(2,1)S(1)} %get-tuple-element.15), channel_id=1, source_target_pairs={{0,3},{1,0},{2,1},{3,2},{4,7},{5,4},{6,5},{7,6},{8,11},{9,8},{10,9... | collective-permute-start | bytes 786440 | tf_op jit(solution)/shard_map/ppermute | solution.py:471
  205.3 13.9 %collective-permute-start.16 = (bf16[64,2048]{1,0:T(8,128)(2,1)S(1)}, bf16[64,2048]{1,0:T(8,128)(2,1)S(1)}, u32[]{:S(2)}, u32[]{:S(2)}) collective-permute-start(bf16[64,2048]{1,0:T(8,128)(2,1)S(1)} %get-tuple-element.16), channel_id=1, source_target_pairs={{0,2},{1,3},{2,0},{3,1},{4,6},{5,7},{6,4},{7,5},{8,10},{9,11},{10,... | collective-permute-start | bytes 786440 | tf_op jit(solution)/shard_map/ppermute | solution.py:472
  (35 other events, 481.0 us)

commit v4 on v3

--- a/solution.py
+++ b/solution.py
@@ -252,7 +252,7 @@
 
 
 def picks_kernel(routes_ref, weight_ref, eight_ref, ninth_ref, scale_ref):
-    experts = ninth_ref.shape[2]
+    experts = ninth_ref.shape[1]
     tokens = routes_ref.shape[1]
     row = lax.broadcasted_iota(jnp.int32, (tokens, tokens), 0)
     col = lax.broadcasted_iota(jnp.int32, (tokens, tokens), 1)
@@ -265,29 +265,44 @@
         place = upright(place.astype(jnp.float32)).astype(jnp.int32)
         eight = lax.broadcasted_iota(jnp.int32, (tokens, experts * 8), 1)
         ninth = lax.broadcasted_iota(jnp.int32, (tokens, experts), 1)
-        eight_ref[k] = as_bf16(eight == jnp.where(place < 8, expert * 8 + place, -1))
-        ninth_ref[k] = as_bf16(ninth == jnp.where(place == 8, expert, -1))
-        scale_ref[k] = jnp.broadcast_to(upright(weight_ref[k : k + 1, :]), scale_ref.shape[1:])
-
-
-def combine_kernel(eight_ref, last_ref, scale_ref, returned_ref, out_ref, ninth_ref):
+        rows = slice(k * tokens, (k + 1) * tokens)
+        eight_ref[rows, :] = as_bf16(eight == jnp.where(place < 8, expert * 8 + place, -1))
+        ninth_ref[rows, :] = as_bf16(ninth == jnp.where(place == 8, expert, -1))
+        scale_ref[rows, :] = jnp.broadcast_to(
+            upright(weight_ref[k : k + 1, :]), (tokens, scale_ref.shape[1])
+        )
+
+
+def combine_kernel(
+    eight_ref, last_ref, scale_ref, returned_ref, out_ref, built_ref, ninth_ref, sems
+):
     experts = returned_ref.shape[0]
     groups = returned_ref.shape[1] // 9
+    tokens = out_ref.shape[0]
     ninth = returned_ref[:, 8 * groups :, :].astype(jnp.float32).reshape(experts * groups, LANES)
     for h in range(LANES // 128):
         ninth_ref[h] = ninth[:, h * 128 : (h + 1) * 128]
+    leaving = []
     for g in range(groups):
         eight = as_rows(returned_ref[:, g * 8 : (g + 1) * 8, :])
         last = jnp.concatenate(
             [ninth_ref[h, pl.ds(g, experts, stride=groups), :] for h in range(LANES // 128)], axis=1
         ).astype(jnp.bfloat16)
-        total = 0.0
-        for k in range(2):
-            chosen = jnp.dot(eight_ref[k], eight, preferred_element_type=jnp.float32) + jnp.dot(
-                last_ref[k], last, preferred_element_type=jnp.float32
-            )
-            total = total + scale_ref[k][:, 0:1] * chosen
-        out_ref[:, g * LANES : (g + 1) * LANES] = total.astype(jnp.bfloat16)
+        chosen = jnp.dot(eight_ref[...], eight, preferred_element_type=jnp.float32) + jnp.dot(
+            last_ref[...], last, preferred_element_type=jnp.float32
+        )
+        scaled = scale_ref[:, 0:1] * chosen
+        columns = pl.ds(g * LANES, LANES)
+        built_ref[:, g * LANES : (g + 1) * LANES] = (scaled[:tokens] + scaled[tokens:]).astype(
+            jnp.bfloat16
+        )
+        copy = pltpu.make_async_copy(
+            built_ref.at[:, columns], out_ref.at[:, columns], sems.at[g]
+        )
+        copy.start()
+        leaving.append(copy)
+    for copy in leaving:
+        copy.wait()
 
 
 def rms_scale(values, gain):
@@ -480,9 +495,9 @@
     masks = pl.pallas_call(
         picks_kernel,
         out_shape=[
-            jax.ShapeDtypeStruct((2, rows_here, ep_count * 8), jnp.bfloat16),
-            jax.ShapeDtypeStruct((2, rows_here, ep_count), jnp.bfloat16),
-            jax.ShapeDtypeStruct((2, rows_here, 128), jnp.float32),
+            jax.ShapeDtypeStruct((2 * rows_here, ep_count * 8), jnp.bfloat16),
+            jax.ShapeDtypeStruct((2 * rows_here, ep_count), jnp.bfloat16),
+            jax.ShapeDtypeStruct((2 * rows_here, 128), jnp.float32),
         ],
         in_specs=[VMEM] * 2,
         out_specs=[VMEM] * 3,
@@ -493,8 +508,12 @@
         combine_kernel,
         out_shape=jax.ShapeDtypeStruct((rows_here, width), jnp.bfloat16),
         in_specs=[VMEM] * 4,
-        out_specs=VMEM,
-        scratch_shapes=[pltpu.VMEM((LANES // 128, ep_count * groups, 128), jnp.float32)],
+        out_specs=HBM,
+        scratch_shapes=[
+            pltpu.VMEM((rows_here, width), jnp.bfloat16),
+            pltpu.VMEM((LANES // 128, ep_count * groups, 128), jnp.float32),
+            pltpu.SemaphoreType.DMA((groups,)),
+        ],
         compiler_params=pltpu.CompilerParams(vmem_limit_bytes=16 * 2**20),
         name="combine_rows",
     )(*[on_chip(m) for m in masks], on_chip(returned))

time: 251 us -> 251 us (level)
  no operation moved by 1% of the time
where the time goes in v4:
time: 251 us; the launch traced here: 247 us
  waiting for transfers between devices  145 us (58%)
  starting transfers between devices  60.3 us (24%)
  Pallas kernels  23.1 us (9%)
  local copies, waits for them, and re-layouts  16.9 us (7%)
    ppermute x7, waiting for transfers between devices, body(): lax.ppermute(keys_values, 'ep', shift_pairs(d, 0, 0))  62 us
    all_to_all x1, waiting for transfers between devices, body(): returned = lax.all_to_all(results, 'ep', 0, 0, tiled=True)  24.4 us
    ppermute x1, waiting for transfers between devices, body(): down_l = lax.ppermute(down, 'tp', to_left)  15.3 us
    unnamed x60, local copies, waits for them, and re-layouts  15.2 us
    ppermute x1, waiting for transfers between devices, body(): gate_l = lax.ppermute(gate, 'tp', to_left)  14.7 us
    ppermute x7, starting transfers between devices, body(): lax.ppermute(keys_values, 'ep', shift_pairs(d, 0, 0))  12.6 us
    all_to_all x1, starting transfers between devices, body(): received = lax.all_to_all(outgoing, 'ep', 0, 0, tiled=True)  12.1 us
    ppermute x1, waiting for transfers between devices, body(): up_f = lax.ppermute(up_l, 'tp', to_left)  11.9 us
  transfers between devices with their start and end apart: 29, of which 18 were waited for; matrix products, arithmetic and copies ran while one was open for 1% of the time, Pallas kernels for 8%

profile of v4, /device:TPU:8, one launch (start us, length us, event | category | flops | bytes accessed | tf_op | source)
XLA Modules:
  0.0 247.2 jit_solution(15183537014035991172)
XLA Ops:
  2.4 2.4 dispatch_rows.1
  4.9 12.1 %all-to-all-start = ((bf16[64,72,256]{2,1,0:T(8,128)(2,1)}), bf16[64,72,256]{2,1,0:T(8,128)(2,1)S(1)}, u32[]{:S(2)}, u32[]{:S(2)}) async-start(bf16[64,72,256]{2,1,0:T(8,128)(2,1)} %dispatch_rows.1), calls=%async_computation | async-start | bytes 4718592 | tf_op jit(solution)/shard_map/all_to_all | solution.py:405
  22.2 2.4 collective-permute-start.1
  24.6 48.7 %collective-permute-done.refs_1_ = bf16[256,128]{1,0:T(8,128)(2,1)S(1)} collective-permute-done((bf16[256,128]{1,0:T(8,128)(2,1)S(1)}, bf16[256,128]{1,0:T(8,128)(2,1)S(1)}, u32[]{:S(2)}, u32[]{:S(2)}) %collective-permute-start) | collective-permute-done | bytes 65568 | tf_op jit(solution)/shard_map/ppermute | solution.py:376
  74.4 2.4 collective-permute-done.1.refs_2_
  78.3 3.0 %collective-permute-done.2.refs_3_ = bf16[256,128]{1,0:T(8,128)(2,1)S(1)} collective-permute-done((bf16[256,128]{1,0:T(8,128)(2,1)S(1)}, bf16[256,128]{1,0:T(8,128)(2,1)S(1)}, u32[]{:S(2)}, u32[]{:S(2)}) %collective-permute-start.2) | collective-permute-done | bytes 65568 | tf_op jit(solution)/shard_map/ppermute | solution.py:376
  81.3 4.2 %collective-permute-start.4 = (bf16[256,128]{1,0:T(8,128)(2,1)S(1)}, bf16[256,128]{1,0:T(8,128)(2,1)S(1)}, u32[]{:S(2)}, u32[]{:S(2)}) collective-permute-start(bf16[256,128]{1,0:T(8,128)(2,1)S(1)} %copy-done.5), channel_id=1, source_target_pairs={{0,160},{4,164},{8,168},{12,172},{16,176},{20,180},{24,184},{28,18... | collective-permute-start | bytes 196616 | tf_op jit(solution)/shard_map/ppermute | solution.py:376
  87.5 3.9 %collective-permute-done.4.refs_5_ = bf16[256,128]{1,0:T(8,128)(2,1)S(1)} collective-permute-done((bf16[256,128]{1,0:T(8,128)(2,1)S(1)}, bf16[256,128]{1,0:T(8,128)(2,1)S(1)}, u32[]{:S(2)}, u32[]{:S(2)}) %collective-permute-start.4) | collective-permute-done | bytes 65568 | tf_op jit(solution)/shard_map/ppermute | solution.py:376
  91.9 3.7 %collective-permute-done.6.refs_7_ = bf16[256,128]{1,0:T(8,128)(2,1)S(1)} collective-permute-done((bf16[256,128]{1,0:T(8,128)(2,1)S(1)}, bf16[256,128]{1,0:T(8,128)(2,1)S(1)}, u32[]{:S(2)}, u32[]{:S(2)}) %collective-permute-start.6) | collective-permute-done | bytes 65568 | tf_op jit(solution)/shard_map/ppermute | solution.py:376
  102.4 15.3 %collective-permute-done.24.d2 = bf16[256,2048]{1,0:T(8,128)(2,1)S(1)} collective-permute-done((bf16[256,2048]{1,0:T(8,128)(2,1)}, bf16[256,2048]{1,0:T(8,128)(2,1)S(1)}, u32[]{:S(2)}, u32[]{:S(2)}) %collective-permute-start.24) | collective-permute-done | bytes 1048608 | tf_op jit(solution)/shard_map/ppermute | solution.py:369
  117.7 2.0 collective-permute-start.7
  122.9 2.5 %collective-permute-start.8 = (bf16[2048,128]{1,0:T(8,128)(2,1)}, bf16[2048,128]{1,0:T(8,128)(2,1)}, u32[]{:S(2)}, u32[]{:S(2)}) collective-permute-start(bf16[2048,128]{1,0:T(8,128)(2,1)} %stack_rows.1.k0), channel_id=1, source_target_pairs={{0,24},{4,28},{8,0},{12,4},{16,8},{20,12},{24,16},{28,20},{32,56},... | collective-permute-start | bytes 1572872 | tf_op jit(solution)/shard_map/ppermute | solution.py:389
  125.5 14.7 %collective-permute-done.19.g2 = bf16[2048,256]{1,0:T(8,128)(2,1)S(1)} collective-permute-done((bf16[2048,256]{1,0:T(8,128)(2,1)S(1)}, bf16[2048,256]{1,0:T(8,128)(2,1)S(1)}, u32[]{:S(2)}, u32[]{:S(2)}) %collective-permute-start.19) | collective-permute-done | bytes 1048608 | tf_op jit(solution)/shard_map/ppermute | solution.py:367
  141.2 3.8 %collective-permute-start.9 = (bf16[2048,128]{1,0:T(8,128)(2,1)}, bf16[2048,128]{1,0:T(8,128)(2,1)}, u32[]{:S(2)}, u32[]{:S(2)}) collective-permute-start(bf16[2048,128]{1,0:T(8,128)(2,1)} %stack_rows.1.k0), channel_id=1, source_target_pairs={{0,16},{4,20},{8,24},{12,28},{16,0},{20,4},{24,8},{28,12},{32,48},... | collective-permute-start | bytes 1572872 | tf_op jit(solution)/shard_map/ppermute | solution.py:389
  147.7 11.9 %collective-permute-done.22.up = bf16[2048,256]{1,0:T(8,128)(2,1)S(1)} collective-permute-done((bf16[2048,256]{1,0:T(8,128)(2,1)S(1)}, bf16[2048,256]{1,0:T(8,128)(2,1)S(1)}, u32[]{:S(2)}, u32[]{:S(2)}) %collective-permute-start.22) | collective-permute-done | bytes 1048608 | tf_op jit(solution)/shard_map/ppermute | solution.py:371
  168.9 4.3 %near_rows.1 = (bf16[576,768]{1,0:T(8,128)(2,1)S(1)}, bf16[576,2048]{1,0:T(8,128)(2,1)S(1)}) custom-call(bf16[64,72,256]{2,1,0:T(8,128)(2,1)S(1)} %all-to-all-done.received_ref, f32[1,2048]{1,0:T(1,128)S(1)} %bitcast.22, bf16[2048,256]{1,0:T(8,128)(2,1)S(1)} %bitcast.15, bf16[2048,256]{1,0:T(8,128)(2,1)S(1)} %bitcast.18, bf16[2048,256]{1,0:T(8,128)(2,1)S(1)} %copy-done.15, ...), custom_call_target="tpu_custom_call" | custom-call | flops 3623878656 | bytes 9000000 | tf_op jit(solution)/shard_map/near_rows/pallas_call | solution.py:406
  173.3 3.2 %far_rows.1 = (bf16[576,256]{1,0:T(8,128)(2,1)S(1)}, f32[576,2048]{1,0:T(8,128)S(1)}) custom-call(bf16[576,2048]{1,0:T(8,128)(2,1)S(1)} %get-tuple-element.20.tokens_ref, bf16[2048,256]{1,0:T(8,128)(2,1)S(1)} %copy-done.23, bf16[2048,256]{1,0:T(8,128)(2,1)S(1)} %copy-done.25, bf16[576,768]{1,0:T(8,128)(2,1)S(1)} %get-tuple-element.21.near_ref, ...), custom_call_target="tpu_custom_call" | custom-call | flops 3019898880 | bytes 9000000 | tf_op jit(solution)/shard_map/far_rows/pallas_call | solution.py:426
  178.5 9.4 %all-to-all-start.1 = ((bf16[64,72,256]{2,1,0:T(8,128)(2,1)}), bf16[64,72,256]{2,1,0:T(8,128)(2,1)S(1)}, u32[]{:S(2)}, u32[]{:S(2)}) async-start(bf16[64,72,256]{2,1,0:T(8,128)(2,1)} %down_rows.1), calls=%async_computation.1 | async-start | bytes 4718592 | tf_op jit(solution)/shard_map/all_to_all | solution.py:463
  193.7 7.8 %attend_rows.1 = (bf16[64,2048]{1,0:T(8,128)(2,1)S(1)}, bf16[64,2048]{1,0:T(8,128)(2,1)S(1)}, bf16[64,2048]{1,0:T(8,128)(2,1)S(1)}, bf16[64,2048]{1,0:T(8,128)(2,1)S(1)}) custom-call(s32[4]{0:T(128)S(1)} %pad_add_fusion.place_ref, bf16[256,256]{1,0:T(8,128)(2,1)S(1)} %copy-done.27, f32[4,16384]{1,0:T(4,128)S(1)} %copy-done.26, ...), custom_call_target="tpu_custom_call" | custom-call | flops 30000001024 | bytes 5000000 | tf_op jit(solution)/shard_map/attend_rows/pallas_call | solution.py:468
  202.9 2.5 %collective-permute-start.15 = (bf16[64,2048]{1,0:T(8,128)(2,1)S(1)}, bf16[64,2048]{1,0:T(8,128)(2,1)S(1)}, u32[]{:S(2)}, u32[]{:S(2)}) collective-permute-start(bf16[64,2048]{1,0:T(8,128)(2,1)S(1)} %get-tuple-element.15), channel_id=1, source_target_pairs={{0,3},{1,0},{2,1},{3,2},{4,7},{5,4},{6,5},{7,6},{8,11},{9,8},{10,9... | collective-permute-start | bytes 786440 | tf_op jit(solution)/shard_map/ppermute | solution.py:486
  207.7 4.7 %collective-permute-done.14 = bf16[64,2048]{1,0:T(8,128)(2,1)S(1)} collective-permute-done((bf16[64,2048]{1,0:T(8,128)(2,1)S(1)}, bf16[64,2048]{1,0:T(8,128)(2,1)S(1)}, u32[]{:S(2)}, u32[]{:S(2)}) %collective-permute-start.14) | collective-permute-done | bytes 262176 | tf_op jit(solution)/shard_map/ppermute | solution.py:485
  212.4 6.8 %collective-permute-done.16 = bf16[64,2048]{1,0:T(8,128)(2,1)S(1)} collective-permute-done((bf16[64,2048]{1,0:T(8,128)(2,1)S(1)}, bf16[64,2048]{1,0:T(8,128)(2,1)S(1)}, u32[]{:S(2)}, u32[]{:S(2)}) %collective-permute-start.16) | collective-permute-done | bytes 262176 | tf_op jit(solution)/shard_map/ppermute | solution.py:487
  220.4 24.4 %all-to-all-done.1.returned_ref = bf16[64,72,256]{2,1,0:T(8,128)(2,1)S(1)} async-done(((bf16[64,72,256]{2,1,0:T(8,128)(2,1)}), bf16[64,72,256]{2,1,0:T(8,128)(2,1)S(1)}, u32[]{:S(2)}, u32[]{:S(2)}) %all-to-all-start.1) | async-done | bytes 2359328 | tf_op jit(solution)/shard_map/all_to_all | solution.py:463
  244.9 2.2 combine_rows.1
  (108 shorter events, 47.7 us)
Async XLA Ops:
  4.9 156.6 %all-to-all-start = ((bf16[64,72,256]{2,1,0:T(8,128)(2,1)}), bf16[64,72,256]{2,1,0:T(8,128)(2,1)S(1)}, u32[]{:S(2)}, u32[]{:S(2)}) async-start(bf16[64,72,256]{2,1,0:T(8,128)(2,1)} %dispatch_rows.1), calls=%async_computation | async-start | bytes 4718592 | tf_op jit(solution)/shard_map/all_to_all | solution.py:405
  17.0 80.3 %collective-permute-start.17 = (bf16[2048,256]{1,0:T(8,128)(2,1)S(1)}, bf16[2048,256]{1,0:T(8,128)(2,1)S(1)}, u32[]{:S(2)}, u32[]{:S(2)}) collective-permute-start(bf16[2048,256]{1,0:T(8,128)(2,1)S(1)} %bitcast.13), channel_id=1, source_target_pairs={{0,1},{1,2},{2,3},{3,0},{4,5},{5,6},{6,7},{7,4},{8,9},{9,10},{10,1... | collective-permute-start | bytes 3145736 | tf_op jit(solution)/shard_map/ppermute | solution.py:364
  18.6 79.1 %collective-permute-start.20 = (bf16[2048,256]{1,0:T(8,128)(2,1)}, bf16[2048,256]{1,0:T(8,128)(2,1)S(1)}, u32[]{:S(2)}, u32[]{:S(2)}) collective-permute-start(bf16[2048,256]{1,0:T(8,128)(2,1)} %bitcast.16), channel_id=1, source_target_pairs={{0,3},{1,0},{2,1},{3,2},{4,7},{5,4},{6,5},{7,6},{8,11},{9,8},{10,9... | collective-permute-start | bytes 3145736 | tf_op jit(solution)/shard_map/ppermute | solution.py:365
  19.1 80.2 %collective-permute-start.23 = (bf16[256,2048]{1,0:T(8,128)(2,1)}, bf16[256,2048]{1,0:T(8,128)(2,1)S(1)}, u32[]{:S(2)}, u32[]{:S(2)}) collective-permute-start(bf16[256,2048]{1,0:T(8,128)(2,1)} %bitcast.19), channel_id=1, source_target_pairs={{0,1},{1,2},{2,3},{3,0},{4,5},{5,6},{6,7},{7,4},{8,9},{9,10},{10,1... | collective-permute-start | bytes 3145736 | tf_op jit(solution)/shard_map/ppermute | solution.py:368
  20.7 52.7 %collective-permute-start = (bf16[256,128]{1,0:T(8,128)(2,1)S(1)}, bf16[256,128]{1,0:T(8,128)(2,1)S(1)}, u32[]{:S(2)}, u32[]{:S(2)}) collective-permute-start(bf16[256,128]{1,0:T(8,128)(2,1)S(1)} %copy-done.5), channel_id=1, source_target_pairs={{0,32},{4,36},{8,40},{12,44},{16,48},{20,52},{24,56},{28,60},{32,6... | collective-permute-start | bytes 196616 | tf_op jit(solution)/shard_map/ppermute | solution.py:376
  22.2 54.6 %collective-permute-start.1 = (bf16[256,128]{1,0:T(8,128)(2,1)S(1)}, bf16[256,128]{1,0:T(8,128)(2,1)S(1)}, u32[]{:S(2)}, u32[]{:S(2)}) collective-permute-start(bf16[256,128]{1,0:T(8,128)(2,1)S(1)} %copy-done.5), channel_id=1, source_target_pairs={{0,64},{4,68},{8,72},{12,76},{16,80},{20,84},{24,88},{28,92},{32,9... | collective-permute-start | bytes 196616 | tf_op jit(solution)/shard_map/ppermute | solution.py:376
  73.4 7.9 %collective-permute-start.2 = (bf16[256,128]{1,0:T(8,128)(2,1)S(1)}, bf16[256,128]{1,0:T(8,128)(2,1)S(1)}, u32[]{:S(2)}, u32[]{:S(2)}) collective-permute-start(bf16[256,128]{1,0:T(8,128)(2,1)S(1)} %copy-done.5), channel_id=1, source_target_pairs={{0,96},{4,100},{8,104},{12,108},{16,112},{20,116},{24,120},{28,124... | collective-permute-start | bytes 196616 | tf_op jit(solution)/shard_map/ppermute | solution.py:376
  76.8 8.8 %collective-permute-start.3 = (bf16[256,128]{1,0:T(8,128)(2,1)S(1)}, bf16[256,128]{1,0:T(8,128)(2,1)S(1)}, u32[]{:S(2)}, u32[]{:S(2)}) collective-permute-start(bf16[256,128]{1,0:T(8,128)(2,1)S(1)} %copy-done.5), channel_id=1, source_target_pairs={{0,128},{4,132},{8,136},{12,140},{16,144},{20,148},{24,152},{28,15... | collective-permute-start | bytes 196616 | tf_op jit(solution)/shard_map/ppermute | solution.py:376
  81.3 10.1 %collective-permute-start.4 = (bf16[256,128]{1,0:T(8,128)(2,1)S(1)}, bf16[256,128]{1,0:T(8,128)(2,1)S(1)}, u32[]{:S(2)}, u32[]{:S(2)}) collective-permute-start(bf16[256,128]{1,0:T(8,128)(2,1)S(1)} %copy-done.5), channel_id=1, source_target_pairs={{0,160},{4,164},{8,168},{12,172},{16,176},{20,180},{24,184},{28,18... | collective-permute-start | bytes 196616 | tf_op jit(solution)/shard_map/ppermute | solution.py:376
  85.6 5.9 %collective-permute-start.5 = (bf16[256,128]{1,0:T(8,128)(2,1)S(1)}, bf16[256,128]{1,0:T(8,128)(2,1)S(1)}, u32[]{:S(2)}, u32[]{:S(2)}) collective-permute-start(bf16[256,128]{1,0:T(8,128)(2,1)S(1)} %copy-done.5), channel_id=1, source_target_pairs={{0,192},{4,196},{8,200},{12,204},{16,208},{20,212},{24,216},{28,22... | collective-permute-start | bytes 196616 | tf_op jit(solution)/shard_map/ppermute | solution.py:376
  91.5 26.2 %collective-permute-start.24 = (bf16[256,2048]{1,0:T(8,128)(2,1)}, bf16[256,2048]{1,0:T(8,128)(2,1)S(1)}, u32[]{:S(2)}, u32[]{:S(2)}) collective-permute-start(bf16[256,2048]{1,0:T(8,128)(2,1)} %bitcast.20), channel_id=1, source_target_pairs={{0,3},{1,0},{2,1},{3,2},{4,7},{5,4},{6,5},{7,6},{8,11},{9,8},{10,9... | collective-permute-start | bytes 3145736 | tf_op jit(solution)/shard_map/ppermute | solution.py:369
  95.7 26.2 %collective-permute-start.18 = (bf16[2048,256]{1,0:T(8,128)(2,1)}, bf16[2048,256]{1,0:T(8,128)(2,1)S(1)}, u32[]{:S(2)}, u32[]{:S(2)}) collective-permute-start(bf16[2048,256]{1,0:T(8,128)(2,1)} %bitcast.17), channel_id=1, source_target_pairs={{0,1},{1,2},{2,3},{3,0},{4,5},{5,6},{6,7},{7,4},{8,9},{9,10},{10,1... | collective-permute-start | bytes 3145736 | tf_op jit(solution)/shard_map/ppermute | solution.py:366
  97.3 42.9 %collective-permute-start.19 = (bf16[2048,256]{1,0:T(8,128)(2,1)S(1)}, bf16[2048,256]{1,0:T(8,128)(2,1)S(1)}, u32[]{:S(2)}, u32[]{:S(2)}) collective-permute-start(bf16[2048,256]{1,0:T(8,128)(2,1)S(1)} %bitcast.14), channel_id=1, source_target_pairs={{0,3},{1,0},{2,1},{3,2},{4,7},{5,4},{6,5},{7,6},{8,11},{9,8},{10,9... | collective-permute-start | bytes 3145736 | tf_op jit(solution)/shard_map/ppermute | solution.py:367
  97.7 47.3 %collective-permute-start.21 = (bf16[2048,256]{1,0:T(8,128)(2,1)S(1)}, bf16[2048,256]{1,0:T(8,128)(2,1)S(1)}, u32[]{:S(2)}, u32[]{:S(2)}) collective-permute-start(bf16[2048,256]{1,0:T(8,128)(2,1)S(1)} %collective-permute-done.17.g1), channel_id=1, source_target_pairs={{0,1},{1,2},{2,3},{3,0},{4,5},{5,6},{6,7},{7,4},{8,9},{9,10},{10,1... | collective-permute-start | bytes 3145736 | tf_op jit(solution)/shard_map/ppermute | solution.py:370
  99.3 60.3 %collective-permute-start.22 = (bf16[2048,256]{1,0:T(8,128)(2,1)S(1)}, bf16[2048,256]{1,0:T(8,128)(2,1)S(1)}, u32[]{:S(2)}, u32[]{:S(2)}) collective-permute-start(bf16[2048,256]{1,0:T(8,128)(2,1)S(1)} %collective-permute-done.20.u2), channel_id=1, source_target_pairs={{0,3},{1,0},{2,1},{3,2},{4,7},{5,4},{6,5},{7,6},{8,11},{9,8},{10,9... | collective-permute-start | bytes 3145736 | tf_op jit(solution)/shard_map/ppermute | solution.py:371
  117.7 70.5 %collective-permute-start.7 = (bf16[2048,128]{1,0:T(8,128)(2,1)}, bf16[2048,128]{1,0:T(8,128)(2,1)}, u32[]{:S(2)}, u32[]{:S(2)}) collective-permute-start(bf16[2048,128]{1,0:T(8,128)(2,1)} %stack_rows.1.k0), channel_id=1, source_target_pairs={{0,8},{4,12},{8,16},{12,20},{16,24},{20,28},{24,0},{28,4},{32,40},... | collective-permute-start | bytes 1572872 | tf_op jit(solution)/shard_map/ppermute | solution.py:389
  122.9 65.8 %collective-permute-start.8 = (bf16[2048,128]{1,0:T(8,128)(2,1)}, bf16[2048,128]{1,0:T(8,128)(2,1)}, u32[]{:S(2)}, u32[]{:S(2)}) collective-permute-start(bf16[2048,128]{1,0:T(8,128)(2,1)} %stack_rows.1.k0), channel_id=1, source_target_pairs={{0,24},{4,28},{8,0},{12,4},{16,8},{20,12},{24,16},{28,20},{32,56},... | collective-permute-start | bytes 1572872 | tf_op jit(solution)/shard_map/ppermute | solution.py:389
  141.2 47.6 %collective-permute-start.9 = (bf16[2048,128]{1,0:T(8,128)(2,1)}, bf16[2048,128]{1,0:T(8,128)(2,1)}, u32[]{:S(2)}, u32[]{:S(2)}) collective-permute-start(bf16[2048,128]{1,0:T(8,128)(2,1)} %stack_rows.1.k0), channel_id=1, source_target_pairs={{0,16},{4,20},{8,24},{12,28},{16,0},{20,4},{24,8},{28,12},{32,48},... | collective-permute-start | bytes 1572872 | tf_op jit(solution)/shard_map/ppermute | solution.py:389
  146.1 30.4 %collective-permute-start.25 = (bf16[128,2048]{1,0:T(8,128)(2,1)}, bf16[128,2048]{1,0:T(8,128)(2,1)S(1)}, u32[]{:S(2)}, u32[]{:S(2)}) collective-permute-start(bf16[128,2048]{1,0:T(8,128)(2,1)} %slice.8), channel_id=1, source_target_pairs={{0,1},{1,2},{2,3},{3,0},{4,5},{5,6},{6,7},{7,4},{8,9},{9,10},{10,1... | collective-permute-start | bytes 1572872 | tf_op jit(solution)/shard_map/ppermute | solution.py:372
  160.5 16.0 %collective-permute-start.26 = (bf16[128,2048]{1,0:T(8,128)(2,1)}, bf16[128,2048]{1,0:T(8,128)(2,1)S(1)}, u32[]{:S(2)}, u32[]{:S(2)}) collective-permute-start(bf16[128,2048]{1,0:T(8,128)(2,1)} %slice.9), channel_id=1, source_target_pairs={{0,3},{1,0},{2,1},{3,2},{4,7},{5,4},{6,5},{7,6},{8,11},{9,8},{10,9... | collective-permute-start | bytes 1572872 | tf_op jit(solution)/shard_map/ppermute | solution.py:373
  178.5 66.3 %all-to-all-start.1 = ((bf16[64,72,256]{2,1,0:T(8,128)(2,1)}), bf16[64,72,256]{2,1,0:T(8,128)(2,1)S(1)}, u32[]{:S(2)}, u32[]{:S(2)}) async-start(bf16[64,72,256]{2,1,0:T(8,128)(2,1)} %down_rows.1), calls=%async_computation.1 | async-start | bytes 4718592 | tf_op jit(solution)/shard_map/all_to_all | solution.py:463
  201.5 10.9 %collective-permute-start.14 = (bf16[64,2048]{1,0:T(8,128)(2,1)S(1)}, bf16[64,2048]{1,0:T(8,128)(2,1)S(1)}, u32[]{:S(2)}, u32[]{:S(2)}) collective-permute-start(bf16[64,2048]{1,0:T(8,128)(2,1)S(1)} %get-tuple-element.14), channel_id=1, source_target_pairs={{0,1},{1,2},{2,3},{3,0},{4,5},{5,6},{6,7},{7,4},{8,9},{9,10},{10,1... | collective-permute-start | bytes 786440 | tf_op jit(solution)/shard_map/ppermute | solution.py:485
  202.9 9.5 %collective-permute-start.15 = (bf16[64,2048]{1,0:T(8,128)(2,1)S(1)}, bf16[64,2048]{1,0:T(8,128)(2,1)S(1)}, u32[]{:S(2)}, u32[]{:S(2)}) collective-permute-start(bf16[64,2048]{1,0:T(8,128)(2,1)S(1)} %get-tuple-element.15), channel_id=1, source_target_pairs={{0,3},{1,0},{2,1},{3,2},{4,7},{5,4},{6,5},{7,6},{8,11},{9,8},{10,9... | collective-permute-start | bytes 786440 | tf_op jit(solution)/shard_map/ppermute | solution.py:486
  205.3 13.9 %collective-permute-start.16 = (bf16[64,2048]{1,0:T(8,128)(2,1)S(1)}, bf16[64,2048]{1,0:T(8,128)(2,1)S(1)}, u32[]{:S(2)}, u32[]{:S(2)}) collective-permute-start(bf16[64,2048]{1,0:T(8,128)(2,1)S(1)} %get-tuple-element.16), channel_id=1, source_target_pairs={{0,2},{1,3},{2,0},{3,1},{4,6},{5,7},{6,4},{7,5},{8,10},{9,11},{10,... | collective-permute-start | bytes 786440 | tf_op jit(solution)/shard_map/ppermute | solution.py:487
  (35 other events, 481.0 us)
